TPU v7x, 128 devices: a whole 4x4x4 slice. The times are simulated.
128 devices in a mesh: ep: 128 (over z, y, x, core).
Axes of the slice: x: 4, y: 4, z: 4, core: 2. Of those that a mesh axis runs over, the one named last changes fastest.
Arguments:
- tokens: bfloat16 [512, 2048], P('ep'), may hold values from -6 to 6
- recurrent_state: float32 [512, 8, 128, 128], P('ep'), may hold values from -4 to 4
- query_weight: bfloat16 [2048, 1024], P(None, 'ep'), may hold values from -0.125 to 0.125
- forget_weight: bfloat16 [2048, 1024], P(None, 'ep'), may hold values from -0.125 to 0.125
- input_weight: bfloat16 [2048, 1024], P(None, 'ep'), may hold values from -0.125 to 0.125
- outgate_weight: bfloat16 [2048, 1024], P(None, 'ep'), may hold values from -0.125 to 0.125
- lower_bound: float32 [1024], replicated, may hold values from 0 to 0.9
- head_gain: float32 [128], replicated, may hold values from 0.1 to 1.9
- mixout_weight: bfloat16 [1024, 2048], P(None, 'ep'), may hold values from -0.1875 to 0.1875
- first_gain: float32 [2048], replicated, may hold values from 0.1 to 1.9
- first_bias: float32 [2048], replicated, may hold values from -1.5 to 1.5
- router_weight: bfloat16 [2048, 8], replicated, may hold values from -0.125 to 0.125
- branch_vector: bfloat16 [2048], replicated, may hold values from -0.125 to 0.125
- dense_gate_weight: bfloat16 [2048, 5632], P(None, 'ep'), may hold values from -0.125 to 0.125
- dense_up_weight: bfloat16 [2048, 5632], P(None, 'ep'), may hold values from -0.125 to 0.125
- dense_down_weight: bfloat16 [5632, 2048], P('ep'), may hold values from -0.078125 to 0.078125
- expert_gate_weight: bfloat16 [2048, 57344], P(None, 'ep'), may hold values from -0.125 to 0.125
- expert_up_weight: bfloat16 [2048, 57344], P(None, 'ep'), may hold values from -0.125 to 0.125
- expert_down_weight: bfloat16 [57344, 2048], P('ep'), may hold values from -0.0625 to 0.0625
- second_gain: float32 [2048], replicated, may hold values from 0.1 to 1.9
- second_bias: float32 [2048], replicated, may hold values from -1.5 to 1.5
- routes: int32 [512, 2], replicated, may hold values from 0 to 7, all different within a row; in each aligned block of 4 rows (0 to 3, 4 to 7, ...) at most 2 rows name the same one
Outputs:
- output: bfloat16 [512, 2048], P('ep')
- new_state: float32 [512, 8, 128, 128], P('ep')
Inputs may be any that keep to these rules, and one draw needn't show every extreme that they name: `routes`: each row names two different experts; in the rows of one device no expert is named more than 2 times, a bound that some block reaches in some device's rows.
All inputs are finite; a program needn't handle non-finite values.
Results may differ from a plain program's by a relative error of at most 0.0095.
Values may be sent and summed in bfloat16 or wider, within the bound.
A program may use at most 64 MiB of HBM per device.

v0:
```python
import jax
import jax.numpy as jnp
from jax import lax
from jax.sharding import Mesh
from jax.sharding import PartitionSpec as P

EXPERTS = 8
B_DEV = 4
CAP = 2
EP = ("ep_0", "ep_1", "ep_2", "ep_3")


ALPHA = 8.0**0.25
NORM_EPS = 1e-05
HEAD_EPS = 1e-06


def from_everyone(shard, axis):
    devices = lax.axis_size(axis)
    return lax.all_to_all(
        jnp.broadcast_to(shard[None], (devices, *shard.shape)), axis, 0, 0, tiled=True
    )


def laid_out(parts, dim):
    dims = list(parts.shape[1:])
    dims[dim] *= parts.shape[0]
    return jnp.moveaxis(parts, 0, dim).reshape(dims)


def gathered_by_axis(shard, axes, dim):
    far, near = axes
    leading = from_everyone(shard, far)
    parts = jnp.swapaxes(from_everyone(leading, near), 0, 1)
    return laid_out(parts.reshape(-1, *shard.shape), dim)


def split_up(shard, dim, devices):
    dims = shard.shape
    parts = shard.reshape(*dims[:dim], devices, dims[dim] // devices, *dims[dim + 1 :])
    return jnp.moveaxis(parts, dim, 0)


def sum_at_owner(shard, axis, dim):
    parts = split_up(shard, dim, lax.axis_size(axis))
    arrived = lax.all_to_all(parts, axis, split_axis=0, concat_axis=0, tiled=True)
    return arrived.astype(jnp.float32).sum(axis=0)


def sum_by_axis(shard, axes, dim):
    far, near = axes
    own = sum_at_owner(split_up(shard, dim, lax.axis_size(far)), near, dim + 1)
    return jnp.sum(
        lax.all_to_all(own.astype(jnp.bfloat16), far, 0, 0, tiled=True).astype(jnp.float32), axis=0
    )


def layer_norm(mixture, gain, bias):
    center = jnp.mean(mixture, axis=-1, keepdims=True)
    spread = jnp.mean(jnp.square(mixture - center), axis=-1, keepdims=True)
    return (mixture - center) * lax.rsqrt(spread + NORM_EPS) * gain + bias


def recurrence(projected, state, lower_bound, head_gain):
    nseq, heads, width = (state.shape[0], state.shape[1], state.shape[2])
    query = projected[:, 0].astype(jnp.float32).reshape(nseq, heads, width)
    forget_in = projected[:, 1].astype(jnp.float32)
    value = projected[:, 2].astype(jnp.float32).reshape(nseq, heads, width)
    outgate = projected[:, 3].astype(jnp.float32)
    forget = (lower_bound + (1.0 - lower_bound) * jax.nn.sigmoid(forget_in)).reshape(
        nseq, heads, width
    )
    keyed = ((1.0 - lower_bound) * jax.nn.sigmoid(-forget_in)).reshape(nseq, heads, width)
    fresh = forget[..., None] * state + keyed[..., None] * value[:, :, None, :]
    read = jnp.einsum("bhkv,bhk->bhv", fresh, query, precision=lax.Precision.HIGHEST)
    scaled = (
        read * lax.rsqrt(jnp.mean(jnp.square(read), axis=-1, keepdims=True) + HEAD_EPS) * head_gain
    )
    mixed = (scaled.reshape(nseq, heads * width) * jax.nn.silu(outgate)).astype(jnp.bfloat16)
    return (mixed, fresh)


def route_share(rows, picks, router_weight):
    f32 = jnp.float32
    logits = jnp.dot(rows, router_weight, preferred_element_type=f32)
    expert_ids = jnp.arange(EXPERTS, dtype=jnp.int32)
    first_logit = jnp.sum(jnp.where(picks[:, 0:1] == expert_ids[None, :], logits, 0.0), axis=1)
    second_logit = jnp.sum(jnp.where(picks[:, 1:2] == expert_ids[None, :], logits, 0.0), axis=1)
    return jax.nn.sigmoid(first_logit - second_logit)


def channel_term(
    with_experts,
    normed_all,
    routes,
    start,
    count,
    router_weight,
    branch_vector,
    dense_gate_weight,
    dense_up_weight,
    dense_down_weight,
    expert_gate_weight,
    expert_up_weight,
    expert_down_weight,
):
    f32 = jnp.float32
    width = normed_all.shape[1]
    branch_gate = jax.nn.sigmoid(jnp.dot(normed_all, branch_vector, preferred_element_type=f32))
    dense_hidden = (
        jax.nn.silu(jnp.dot(normed_all, dense_gate_weight, preferred_element_type=f32))
        * jnp.dot(normed_all, dense_up_weight, preferred_element_type=f32)
    ).astype(jnp.bfloat16)
    dense_part = branch_gate[:, None] * jnp.dot(
        dense_hidden, dense_down_weight, preferred_element_type=f32
    )
    share = route_share(normed_all, routes, router_weight)
    spread_count = lax.axis_size(EP) // EXPERTS
    expert = lax.axis_index(EP) // spread_count
    on_first = routes[:, 0] == expert
    on_second = routes[:, 1] == expert
    token_weight = share * on_first.astype(f32) + (1.0 - share) * on_second.astype(f32)
    sources = count // B_DEV
    hits = (on_first | on_second).astype(jnp.int32).reshape(sources, B_DEV)
    ranks = jnp.cumsum(hits, axis=1) - 1
    slot_ids = jnp.arange(CAP, dtype=jnp.int32)
    select = (ranks[:, None, :] == slot_ids[None, :, None]) & (hits[:, None, :] > 0)
    slot_rows = (
        jnp.einsum(
            "sci,sid->scd",
            select.astype(jnp.bfloat16),
            normed_all.reshape(sources, B_DEV, width),
            preferred_element_type=f32,
        )
        .astype(jnp.bfloat16)
        .reshape(sources * CAP, width)
    )
    gate_part = jnp.dot(slot_rows, expert_gate_weight, preferred_element_type=f32)
    up_part = jnp.dot(slot_rows, expert_up_weight, preferred_element_type=f32)
    hidden = (jax.nn.silu(gate_part) * up_part).astype(jnp.bfloat16)
    slot_out = jnp.dot(hidden, expert_down_weight, preferred_element_type=f32).reshape(
        sources, CAP, width
    )
    back = jnp.einsum("sci,scd->sid", select.astype(f32), slot_out, precision=lax.Precision.HIGHEST)
    return back.reshape(count, width) * token_weight[:, None] + dense_part


def per_device(
    tokens,
    recurrent_state,
    query_weight,
    forget_weight,
    input_weight,
    outgate_weight,
    lower_bound,
    head_gain,
    mixout_weight,
    first_gain,
    first_bias,
    router_weight,
    branch_vector,
    dense_gate_weight,
    dense_up_weight,
    dense_down_weight,
    expert_gate_weight,
    expert_up_weight,
    expert_down_weight,
    second_gain,
    second_bias,
    routes,
):
    f32 = jnp.float32
    devices = lax.axis_size(EP)
    nseq, width = tokens.shape
    own_cols = query_weight.shape[1]
    stacked = jnp.concatenate([query_weight, forget_weight, input_weight, outgate_weight], axis=1)
    weights = (
        router_weight,
        branch_vector,
        dense_gate_weight,
        dense_up_weight,
        dense_down_weight,
        expert_gate_weight,
        expert_up_weight,
        expert_down_weight,
    )
    gathered = jnp.dot(
        gathered_by_axis(tokens, (("ep_0", "ep_1", "ep_2"), "ep_3"), 0),
        stacked,
        preferred_element_type=f32,
    ).astype(jnp.bfloat16)
    owned = lax.all_to_all(gathered, EP, split_axis=0, concat_axis=1, tiled=True)
    projected = (
        owned.reshape(nseq, devices, 4, own_cols)
        .transpose(0, 2, 1, 3)
        .reshape(nseq, 4, devices * own_cols)
    )
    mixed, new_state = recurrence(projected, recurrent_state, lower_bound, head_gain)
    mix_cols = jnp.dot(
        gathered_by_axis(mixed, (("ep_0", "ep_1", "ep_2"), "ep_3"), 0),
        mixout_weight,
        preferred_element_type=f32,
    ).astype(jnp.bfloat16)
    mix_out = lax.all_to_all(mix_cols, EP, split_axis=0, concat_axis=1, tiled=True)
    normed = layer_norm(
        ALPHA * tokens.astype(f32) + mix_out.astype(f32), first_gain, first_bias
    ).astype(jnp.bfloat16)
    normed_all = gathered_by_axis(normed, (("ep_0", "ep_1", "ep_2"), "ep_3"), 0)
    channel = sum_by_axis(
        channel_term(
            True, normed_all, routes, jnp.int32(0), nseq * lax.axis_size(EP), *weights
        ).astype(jnp.bfloat16),
        (("ep_0", "ep_1", "ep_2"), "ep_3"),
        0,
    )
    output = layer_norm(ALPHA * normed.astype(f32) + channel, second_gain, second_bias).astype(
        jnp.bfloat16
    )
    return (output, new_state)


def solution(mesh):
    finer = Mesh(mesh.devices.reshape(4, 4, 4, 2), ("ep_0", "ep_1", "ep_2", "ep_3"))
    return jax.shard_map(
        per_device,
        mesh=finer,
        in_specs=(
            P(EP, None),
            P(EP, None, None, None),
            P(None, EP),
            P(None, EP),
            P(None, EP),
            P(None, EP),
            P(),
            P(),
            P(None, EP),
            P(),
            P(),
            P(),
            P(),
            P(None, EP),
            P(None, EP),
            P(EP, None),
            P(None, EP),
            P(None, EP),
            P(EP, None),
            P(),
            P(),
            P(),
        ),
        out_specs=(P(EP, None), P(EP, None, None, None)),
        check_vma=False,
    )
```

profile of v0, /device:TPU:0, one launch (start us, length us, event | category | flops | bytes accessed | tf_op | source)
XLA Modules:
  0.0 230.2 jit_solution(17035206795366007720)
XLA Ops:
  2.0 30.2 %all_to_all.69 = bf16[64,4,2048]{2,1,0:T(4,128)(2,1)S(1)} all-to-all(bf16[64,4,2048]{2,1,0:T(4,128)(2,1)S(1)} %broadcast_in_dim.16), channel_id=1, replica_groups=mesh['ep_0'=4,'ep_1'=4,'ep_2'=4,'ep_3'=2] {'ep_0','ep_1','ep_2'}, dimensions={0} | all-to-all | bytes 2097152 | tf_op jit(solution)/shard_map/all_to_all | solution.py:20
  33.3 5.4 %all_to_all.70 = bf16[2,64,4,2048]{3,2,1,0:T(4,128)(2,1)S(1)} all-to-all(bf16[2,64,4,2048]{3,2,1,0:T(4,128)(2,1)S(1)} %broadcast_in_dim.17), channel_id=1, replica_groups=mesh['ep_0'=4,'ep_1'=4,'ep_2'=4,'ep_3'=2] {'ep_3'}, dimensions={0} | all-to-all | bytes 4194304 | tf_op jit(solution)/shard_map/all_to_all | solution.py:20
  38.7 2.7 %copy.74 = bf16[64,2,4,2048]{3,2,1,0:T(4,128)(2,1)} copy(bf16[64,2,4,2048]{3,2,0,1:T(4,128)(2,1)S(1)} %bitcast.73) | data formatting | bytes 4194304 | tf_op jit(solution)/shard_map/transpose | solution.py:34
  41.5 4.0 %reshape_reshape.12 = bf16[512,2048]{1,0:T(8,128)(2,1)} reshape(bf16[64,2,4,2048]{3,2,1,0:T(4,128)(2,1)} %copy.74) | data formatting | bytes 4194304 | tf_op jit(solution)/shard_map/reshape;reshape | solution.py:28
  48.6 4.6 %all-to-all-start.2 = ((bf16[128,4,32]{2,1,0:T(4,128)(2,1)}), bf16[128,4,32]{2,1,0:T(4,128)(2,1)S(1)}, u32[]{:S(2)}, u32[]{:S(2)}) async-start(bf16[128,4,32]{2,1,0:T(4,128)(2,1)} %bitcast.4), calls=%async_computation.2 | async-start | bytes 262144 | tf_op jit(solution)/shard_map/all_to_all | solution.py:192
  53.2 9.4 %all-to-all-done.2 = bf16[128,4,32]{2,1,0:T(4,128)(2,1)S(1)} async-done(((bf16[128,4,32]{2,1,0:T(4,128)(2,1)}), bf16[128,4,32]{2,1,0:T(4,128)(2,1)S(1)}, u32[]{:S(2)}, u32[]{:S(2)}) %all-to-all-start.2) | async-done | bytes 32800 | tf_op jit(solution)/shard_map/all_to_all | solution.py:192
  68.9 18.4 %all_to_all.71 = bf16[64,4,1024]{2,1,0:T(4,128)(2,1)S(1)} all-to-all(bf16[64,4,1024]{2,1,0:T(4,128)(2,1)S(1)} %broadcast_in_dim.18), channel_id=1, replica_groups=mesh['ep_0'=4,'ep_1'=4,'ep_2'=4,'ep_3'=2] {'ep_0','ep_1','ep_2'}, dimensions={0} | all-to-all | bytes 1048576 | tf_op jit(solution)/shard_map/all_to_all | solution.py:20
  87.6 4.6 %all_to_all.72 = bf16[2,64,4,1024]{3,2,1,0:T(4,128)(2,1)S(1)} all-to-all(bf16[2,64,4,1024]{3,2,1,0:T(4,128)(2,1)S(1)} %broadcast_in_dim.19), channel_id=1, replica_groups=mesh['ep_0'=4,'ep_1'=4,'ep_2'=4,'ep_3'=2] {'ep_3'}, dimensions={0} | all-to-all | bytes 2097152 | tf_op jit(solution)/shard_map/all_to_all | solution.py:20
  95.7 13.9 %all_to_all.73 = bf16[128,4,16]{2,1,0:T(4,128)(2,1)S(1)} all-to-all(bf16[128,4,16]{2,1,0:T(4,128)(2,1)S(1)} %bitcast.78), channel_id=1, replica_groups=mesh['ep_0'=4,'ep_1'=4,'ep_2'=4,'ep_3'=2] {'ep_0','ep_1','ep_2','ep_3'}, dimensions={0} | all-to-all | bytes 32768 | tf_op jit(solution)/shard_map/all_to_all | solution.py:204
  111.8 5.1 %all-to-all-start.6 = ((bf16[64,4,2048]{2,1,0:T(4,128)(2,1)}), bf16[64,4,2048]{2,1,0:T(4,128)(2,1)S(1)}, u32[]{:S(2)}, u32[]{:S(2)}) async-start(bf16[64,4,2048]{2,1,0:T(4,128)(2,1)} %broadcast_in_dim.20), calls=%async_computation.6 | async-start | bytes 2097152 | tf_op jit(solution)/shard_map/all_to_all | solution.py:20
  117.3 18.5 %all-to-all-done.6 = bf16[64,4,2048]{2,1,0:T(4,128)(2,1)S(1)} async-done(((bf16[64,4,2048]{2,1,0:T(4,128)(2,1)}), bf16[64,4,2048]{2,1,0:T(4,128)(2,1)S(1)}, u32[]{:S(2)}, u32[]{:S(2)}) %all-to-all-start.6) | async-done | bytes 1048608 | tf_op jit(solution)/shard_map/all_to_all | solution.py:20
  136.8 5.4 %all_to_all.74 = bf16[2,64,4,2048]{3,2,1,0:T(4,128)(2,1)S(1)} all-to-all(bf16[2,64,4,2048]{3,2,1,0:T(4,128)(2,1)S(1)} %broadcast_in_dim.21), channel_id=1, replica_groups=mesh['ep_0'=4,'ep_1'=4,'ep_2'=4,'ep_3'=2] {'ep_3'}, dimensions={0} | all-to-all | bytes 4194304 | tf_op jit(solution)/shard_map/all_to_all | solution.py:20
  142.3 2.8 %copy.81 = bf16[64,2,4,2048]{3,2,1,0:T(4,128)(2,1)} copy(bf16[64,2,4,2048]{3,2,0,1:T(4,128)(2,1)S(1)} %bitcast.74) | data formatting | bytes 4194304 | tf_op jit(solution)/shard_map/transpose | solution.py:34
  145.0 4.0 %reshape_reshape.14 = bf16[512,2048]{1,0:T(8,128)(2,1)} reshape(bf16[64,2,4,2048]{3,2,1,0:T(4,128)(2,1)} %copy.81) | data formatting | bytes 4194304 | tf_op jit(solution)/shard_map/reshape;reshape | solution.py:28
  157.4 5.1 %fusion.1 = f32[256,2048]{1,0:T(8,128)} fusion(bf16[448,2048]{1,0:T(8,128)(2,1)S(1)} %copy-done, bf16[256,2048]{1,0:T(8,128)(2,1)S(1)} %reshape.239, bf16[2048,448]{0,1:T(8,128)(2,1)} %param.39, f32[256,448]{0,1:T(8,128)S(1)} %fusion.41), kind=kOutput, calls=%fused_computation.7 | convolution fusion | flops 940212224 | bytes 7274496 | tf_op jit(solution)/shard_map/dot_general | solution.py:141
  162.4 3.5 %reshape.240 = f32[128,2,2048]{2,1,0:T(2,128)} reshape(f32[256,2048]{1,0:T(8,128)} %fusion.1) | data formatting | bytes 4194304 | tf_op jit(solution)/shard_map/reshape | solution.py:141
  165.9 7.8 %fusion.17 = f32[128,4,2048]{2,1,0:T(4,128)} fusion(f32[128,2,2048]{2,1,0:T(2,128)} %reshape.240, pred[128,4]{1,0:T(8,128)(4,1)S(1)} %broadcast_compare_fusion, s32[128,4]{1,0:T(8,128)S(1)} %broadcast_add_fusion), kind=kOutput, calls=%fused_computation.28 | convolution fusion | flops 25167872 | bytes 6294016 | tf_op jit(solution)/shard_map/sci,scd->sid/dot_general | solution.py:144
  173.8 5.3 %reshape.241 = f32[512,2048]{1,0:T(8,128)} reshape(f32[128,4,2048]{2,1,0:T(4,128)} %fusion.17) | data formatting | bytes 8388608 | tf_op jit(solution)/shard_map/reshape | solution.py:145
  182.3 5.7 %add_convert_fusion = bf16[512,2048]{1,0:T(8,128)(2,1)} fusion(f32[512,2048]{1,0:T(8,128)} %reshape.241, bf16[44,2048]{1,0:T(8,128)(2,1)S(1)} %copy-done.6, f32[512]{0:T(512)S(1)} %add_divide_fusion.2, f32[512]{0:T(512)S(1)} %bitcast.90, bf16[512,2048]{1,0:T(8,128)(2,1)} %reshape_reshape.14, bf16[2048,44]{0,1:T(8,128)(2,1)S(1)} %copy-done.7, ...), kind=kOutput, calls=%fused_computation | convolution fusion | flops 188878848 | bytes 8843264 | tf_op jit(solution)/shard_map/dot_general | solution.py:114
  188.0 4.1 %reshape_reshape.15 = bf16[64,2,4,2048]{3,2,1,0:T(4,128)(2,1)} reshape(bf16[512,2048]{1,0:T(8,128)(2,1)} %add_convert_fusion) | data formatting | bytes 4194304 | tf_op jit(solution)/shard_map/reshape;reshape | solution.py:40
  192.1 2.8 %copy.97 = bf16[64,2,4,2048]{3,2,0,1:T(4,128)(2,1)S(1)} copy(bf16[64,2,4,2048]{3,2,1,0:T(4,128)(2,1)} %reshape_reshape.15) | data formatting | bytes 4194304 | tf_op jit(solution)/shard_map/reshape;reshape | solution.py:40
  194.8 6.3 %all_to_all.75 = bf16[2,64,4,2048]{3,2,1,0:T(4,128)(2,1)} all-to-all(bf16[2,64,4,2048]{3,2,1,0:T(4,128)(2,1)S(1)} %bitcast.75), channel_id=1, replica_groups=mesh['ep_0'=4,'ep_1'=4,'ep_2'=4,'ep_3'=2] {'ep_3'}, dimensions={0} | all-to-all | bytes 4194304 | tf_op jit(solution)/shard_map/all_to_all | solution.py:46
  201.2 3.6 %reduce_sum.89 = bf16[64,4,2048]{2,1,0:T(4,128)(2,1)S(1)} reduce(bf16[2,64,4,2048]{3,2,1,0:T(4,128)(2,1)} %all_to_all.75, bf16[]{:T(256)} %constant.73.clone.1), dimensions={0}, to_apply=%region_6.7 | reduce | flops 524288 | bytes 3145730 | tf_op jit(solution)/shard_map/reduce_sum | solution.py:47
  204.8 23.7 %all_to_all.76 = bf16[64,4,2048]{2,1,0:T(4,128)(2,1)S(1)} all-to-all(bf16[64,4,2048]{2,1,0:T(4,128)(2,1)S(1)} %reduce_sum.89), channel_id=1, replica_groups=mesh['ep_0'=4,'ep_1'=4,'ep_2'=4,'ep_3'=2] {'ep_0','ep_1','ep_2'}, dimensions={0} | all-to-all | bytes 2097152 | tf_op jit(solution)/shard_map/all_to_all | solution.py:54
  (98 shorter events, 32.2 us)
Async XLA Ops:
  0.6 156.7 %copy-start = (bf16[448,2048]{1,0:T(8,128)(2,1)S(1)}, bf16[448,2048]{1,0:T(8,128)(2,1)}, u32[]{:S(2)}) copy-start(bf16[448,2048]{1,0:T(8,128)(2,1)} %param.40) | copy-start | bytes 5505028
  41.4 4.0 %copy-start.8 = (bf16[2048,8]{0,1:T(8,128)(2,1)S(1)}, bf16[2048,8]{0,1:T(8,128)(2,1)}, u32[]{:S(2)}) copy-start(bf16[2048,8]{0,1:T(8,128)(2,1)} %param.27) | copy-start | bytes 98308
  41.4 4.0 %copy-start.9 = (bf16[2048,8]{0,1:T(8,128)(2,1)S(1)}, bf16[2048,8]{0,1:T(8,128)(2,1)}, u32[]{:S(2)}) copy-start(bf16[2048,8]{0,1:T(8,128)(2,1)} %param.26) | copy-start | bytes 98308
  41.4 4.0 %copy-start.10 = (bf16[2048,8]{0,1:T(8,128)(2,1)S(1)}, bf16[2048,8]{0,1:T(8,128)(2,1)}, u32[]{:S(2)}) copy-start(bf16[2048,8]{0,1:T(8,128)(2,1)} %param.25) | copy-start | bytes 98308
  41.4 4.0 %copy-start.11 = (bf16[2048,8]{0,1:T(8,128)(2,1)S(1)}, bf16[2048,8]{0,1:T(8,128)(2,1)}, u32[]{:S(2)}) copy-start(bf16[2048,8]{0,1:T(8,128)(2,1)} %param.24) | copy-start | bytes 98308
  45.5 7.7 %copy-start.14 = (f32[1024]{0:T(1024)S(1)}, f32[1024]{0:T(1024)}, u32[]{:S(2)}) copy-start(f32[1024]{0:T(1024)} %param.28) | copy-start | bytes 12292
  48.6 14.0 %all-to-all-start.2 = ((bf16[128,4,32]{2,1,0:T(4,128)(2,1)}), bf16[128,4,32]{2,1,0:T(4,128)(2,1)S(1)}, u32[]{:S(2)}, u32[]{:S(2)}) async-start(bf16[128,4,32]{2,1,0:T(4,128)(2,1)} %bitcast.4), calls=%async_computation.2 | async-start | bytes 262144 | tf_op jit(solution)/shard_map/all_to_all | solution.py:192
  66.2 1.3 copy-start.2
  67.5 1.2 copy-start.21
  92.2 1.7 copy-start.13
  92.8 17.0 %copy-start.4 = (bf16[4,2048]{1,0:T(4,128)(2,1)S(1)}, bf16[4,2048]{1,0:T(4,128)(2,1)}, u32[]{:S(2)}) copy-start(bf16[4,2048]{1,0:T(4,128)(2,1)} %param.22) | copy-start | bytes 49156
  92.8 17.4 %copy-start.16 = (f32[2048]{0:T(1024)S(1)}, f32[2048]{0:T(1024)}, u32[]{:S(2)}) copy-start(f32[2048]{0:T(1024)} %param.32) | copy-start | bytes 24580
  92.8 17.4 %copy-start.17 = (f32[2048]{0:T(1024)S(1)}, f32[2048]{0:T(1024)}, u32[]{:S(2)}) copy-start(f32[2048]{0:T(1024)} %param.31) | copy-start | bytes 24580
  109.6 7.3 %copy-start.15 = (s32[512,2]{0,1:T(2,128)S(1)}, s32[512,2]{0,1:T(2,128)}, u32[]{:S(2)}) copy-start(s32[512,2]{0,1:T(2,128)} %param.43) | copy-start | bytes 12292
  109.6 7.7 %copy-start.20 = (bf16[2048]{0:T(1024)(128)(2,1)S(1)}, bf16[2048]{0:T(1024)(128)(2,1)}, u32[]{:S(2)}) copy-start(bf16[2048]{0:T(1024)(128)(2,1)} %param.34) | copy-start | bytes 12292
  111.8 24.0 %all-to-all-start.6 = ((bf16[64,4,2048]{2,1,0:T(4,128)(2,1)}), bf16[64,4,2048]{2,1,0:T(4,128)(2,1)S(1)}, u32[]{:S(2)}, u32[]{:S(2)}) async-start(bf16[64,4,2048]{2,1,0:T(4,128)(2,1)} %broadcast_in_dim.20), calls=%async_computation.6 | async-start | bytes 2097152 | tf_op jit(solution)/shard_map/all_to_all | solution.py:20
  145.0 4.0 %copy-start.12 = (bf16[2048,8]{0,1:T(8,128)(2,1)S(1)}, bf16[2048,8]{0,1:T(8,128)(2,1)}, u32[]{:S(2)}) copy-start(bf16[2048,8]{0,1:T(8,128)(2,1)} %param.33) | copy-start | bytes 98308
  149.0 2.4 %copy-start.3 = (bf16[64,2,4,2048]{3,2,1,0:T(4,128)(2,1)S(1)}, bf16[64,2,4,2048]{3,2,1,0:T(4,128)(2,1)}, u32[]{:S(2)}) copy-start(bf16[64,2,4,2048]{3,2,1,0:T(4,128)(2,1)} %copy.81) | copy-start | bytes 6291460
  173.8 5.3 %copy-start.5 = (bf16[2048,44]{0,1:T(8,128)(2,1)S(1)}, bf16[2048,44]{0,1:T(8,128)(2,1)}, u32[]{:S(2)}) copy-start(bf16[2048,44]{0,1:T(8,128)(2,1)} %param.35) | copy-start | bytes 540676
  179.1 2.5 %copy-start.1 = (bf16[512,2048]{1,0:T(8,128)(2,1)S(1)}, bf16[512,2048]{1,0:T(8,128)(2,1)}, u32[]{:S(2)}) copy-start(bf16[512,2048]{1,0:T(8,128)(2,1)} %reshape_reshape.14) | copy-start | bytes 6291460
  179.1 3.2 %copy-start.6 = (bf16[44,2048]{1,0:T(8,128)(2,1)S(1)}, bf16[44,2048]{1,0:T(8,128)(2,1)}, u32[]{:S(2)}) copy-start(bf16[44,2048]{1,0:T(8,128)(2,1)} %param.37) | copy-start | bytes 540676
  179.1 3.2 %copy-start.7 = (bf16[2048,44]{0,1:T(8,128)(2,1)S(1)}, bf16[2048,44]{0,1:T(8,128)(2,1)}, u32[]{:S(2)}) copy-start(bf16[2048,44]{0,1:T(8,128)(2,1)} %param.36) | copy-start | bytes 540676
  204.7 24.7 %copy-start.18 = (f32[2048]{0:T(1024)S(1)}, f32[2048]{0:T(1024)}, u32[]{:S(2)}) copy-start(f32[2048]{0:T(1024)} %param.42) | copy-start | bytes 24580
  204.8 24.7 %copy-start.19 = (f32[2048]{0:T(1024)S(1)}, f32[2048]{0:T(1024)}, u32[]{:S(2)}) copy-start(f32[2048]{0:T(1024)} %param.41) | copy-start | bytes 24580
where the time goes:
time: 231 us; the launch traced here: 230 us
  blocking collectives  108 us (47%)
  local copies, waits for them, and re-layouts  41.3 us (18%)
  matrix products  33.5 us (15%)
  waiting for transfers between devices  27.8 us (12%)
  starting transfers between devices  9.75 us (4%)
  other arithmetic  8.75 us (4%)
    all_to_all x5, blocking collectives, from_everyone(): lax.all_to_all(jnp.broadcast_to(shard[None], (devices, *shard.shape)), ax...  64.1 us
    all_to_all x1, blocking collectives, sum_by_axis(): lax.all_to_all(own.astype(jnp.bfloat16), far, 0, 0, tiled=True)  23.7 us
    all_to_all x1, waiting for transfers between devices, from_everyone(): lax.all_to_all(jnp.broadcast_to(shard[None], (devices, *shard.shape)), ax...  18.5 us
    all_to_all x1, blocking collectives, per_device(): lax.all_to_all(mix_cols, EP, split_axis=0, concat_axis=1, tiled=True)  13.9 us
    all_to_all x1, waiting for transfers between devices, per_device(): lax.all_to_all(gathered, EP, split_axis=0, concat_axis=1, tiled=True)  9.36 us
    another operation x3, local copies, waits for them, and re-layouts, laid_out(): return jnp.moveaxis(parts, 0, dim).reshape(dims)  9.11 us
    dot_general x1, matrix products, channel_term(): jnp.einsum('sci,scd->sid', select.astype(f32), slot_out, precision=lax.Pr...  7.84 us
    another operation x2, local copies, waits for them, and re-layouts, split_up(): shard.reshape(*dims[:dim], devices, dims[dim] // devices, *dims[dim + 1:])  6.87 us
  transfers between devices with their start and end apart: 2, of which 2 were waited for; matrix products, arithmetic and copies ran while one was open for 0% of the time, Pallas kernels for 0%

commit v1 on v0

v1 whole, which is shorter than its diff:
```python
import functools

import jax
import jax.numpy as jnp
from jax import lax
from jax.experimental import pallas as pl
from jax.experimental.pallas import tpu as pltpu
from jax.sharding import PartitionSpec as P

ALPHA = 8.0**0.25
NORM_EPS = 1e-05
HEAD_EPS = 1e-06
HALF = 1024
F32 = jnp.float32
BF16 = jnp.bfloat16
PARTS = (
    (slice(0, 384), (2, 1, 0)),
    (slice(384, 768), (1, 0, 2)),
    (slice(768, 1024), (0, 2, 1)),
)
NT = (((1,), (1,)), ((), ()))


def dot(a, b):
    return jnp.dot(a, b, preferred_element_type=F32)


def dot_nt(a, b):
    return lax.dot_general(a, b, NT, preferred_element_type=F32)


def iota(shape, dim):
    return lax.broadcasted_iota(jnp.int32, shape, dim)


def sigmoid(a):
    return 1.0 / (1.0 + jnp.exp(-a))


def kernel(
    tok_h, state_h, wq_h, wf_h, wi_h, wo_h, lb_h, hg_h, wm_h, g1_h, b1_h, router_h, branch_h,
    dg_h, du_h, dd_h, eg_h, eu_h, ed_h, g2_h, b2_h, routes_h,
    out_ref, nst_h,
    tokv, st, nst, wp, lb, hg, wm, g1, b1, rt, br, dg, du, dd, eg, eu, ed, g2, b2, rts,
    tb, nb, msg, rcv, ob, xe, wd, wdd, rd,
    r1a, r1b, r1c, r2a, r2b, r2c, r3a, r3b, r3c, t1a, t1b, t1c, t2a, t2b, t2c,
    loc, stsem, nsem, pw_s, pw_r, wm_s, wm_r, wmx_s, wmx_r, tk_s, tk_r, nb_s, nb_r, a2_s, a2_r, rs_s, rs_r,
):
    me = lax.axis_index("ep")
    core = me % 2
    chip = me // 2
    at = (chip // 16, (chip // 4) % 4, chip % 4)
    partner = me + 1 - 2 * core

    def peer(dim, k):
        c = [at[0], at[1], at[2]]
        c[dim] = (c[dim] + k) % 4
        return 2 * ((c[0] * 4 + c[1]) * 4 + c[2]) + core

    def remote(src, dst, ss, rs, dev):
        pltpu.make_async_remote_copy(
            src_ref=src, dst_ref=dst, send_sem=ss, recv_sem=rs, device_id=(dev,),
            device_id_type=pl.DeviceIdType.MESH,
        ).start()

    def local(src, dst, sem):
        cp = pltpu.make_async_copy(src, dst, sem)
        cp.start()
        return cp

    def take(ref, sem):
        pltpu.make_async_copy(ref, ref, sem).wait()

    own = (at[0], at[1], at[2])
    c_tok = local(tok_h, tokv, loc.at[0])
    c_wp = [local(w, wp.at[i, core], loc.at[1 + i]) for i, w in enumerate((wq_h, wf_h, wi_h, wo_h))]
    c_wm = local(wm_h, wm.at[own + (core,)], loc.at[5])
    c_small = [
        local(a, b, loc.at[6 + i])
        for i, (a, b) in enumerate(
            ((lb_h, lb), (hg_h, hg), (g1_h, g1), (b1_h, b1), (router_h, rt), (branch_h, br),
             (g2_h, g2), (b2_h, b2), (routes_h, rts))
        )
    ]
    barrier = pltpu.get_barrier_semaphore()
    for dim in range(3):
        for k in range(1, 4):
            pl.semaphore_signal(barrier, inc=1, device_id=(peer(dim, k),), device_id_type=pl.DeviceIdType.MESH)
    pl.semaphore_signal(barrier, inc=1, device_id=(partner,), device_id_type=pl.DeviceIdType.MESH)
    c_tok.wait()
    toks = tokv[...].astype(F32)
    tblk = jnp.concatenate([toks[:, :HALF], toks[:, HALF:]], axis=0).astype(BF16)
    tb[own] = tblk
    pl.semaphore_wait(barrier, 10)

    def ag_send(buf, tail, part, phase, ss, rs):
        lanes, order = PARTS[part]
        idx = tuple(slice(None) if d in order[:phase] else at[d] for d in range(3))
        ref = buf.at[idx + tail + (slice(None), lanes)]
        for k in (2, 1, 3):
            remote(ref, ref, ss.at[part, phase], rs.at[part, phase], peer(order[phase], k))

    def three(buf, tail, part, phase):
        lanes, _ = PARTS[part]
        idx = ((0, 0, slice(0, 3)), (0, slice(0, 3), slice(None)), (slice(0, 3), slice(None), slice(None)))[phase]
        return buf.at[idx + tail + (slice(None), lanes)]

    def ag_take(buf, tail, part, phase, rs):
        take(three(buf, tail, part, phase), rs.at[part, phase])

    for part in range(3):
        ag_send(tb, (), part, 0, tk_s, tk_r)
    for i, w in enumerate((wq_h, wf_h, wi_h, wo_h)):
        remote(w, wp.at[i, core], pw_s.at[i], pw_r.at[i], partner)
    wtail = (core,)
    c_wm.wait()
    for part in range(3):
        ag_send(wm, wtail, part, 0, wm_s, wm_r)
    c_st = [local(state_h.at[t], st.at[t], stsem.at[t]) for t in range(4)]
    c_w = []
    for i, (a, b) in enumerate(((dg_h, dg), (du_h, du), (dd_h, dd), (eg_h, eg), (eu_h, eu), (ed_h, ed))):
        c_w.append(local(a, b.at[core], loc.at[15 + i]))
    for part in range(3):
        ag_take(tb, (), part, 0, tk_r)
        ag_send(tb, (), part, 1, tk_s, tk_r)
    for part in range(3):
        ag_take(wm, wtail, part, 0, wm_r)
        ag_send(wm, wtail, part, 1, wm_s, wm_r)
    for part in range(3):
        ag_take(tb, (), part, 1, tk_r)
        ag_send(tb, (), part, 2, tk_s, tk_r)
    for i, (a, b) in enumerate(((dg_h, dg), (du_h, du), (dd_h, dd), (eg_h, eg), (eu_h, eu), (ed_h, ed))):
        remote(a, b.at[core], pw_s.at[4 + i], pw_r.at[4 + i], partner)

    for c in c_small:
        c.wait()
    expert = chip // 8
    r0 = rts[0:1, :]
    r1 = rts[1:2, :]
    lane = iota((1, 512), 1)
    hit = jnp.where((r0 == expert) | (r1 == expert), 1.0, 0.0)
    other = jnp.where(r0 == expert, r1, r0).astype(F32)
    mine = (lane // 4) % 2 == core

    def own_rows(v):
        moved = jnp.where(core == 0, pltpu.roll(v, 4, 1), pltpu.roll(v, 508, 1))
        return jnp.where(mine, v, moved)

    hit = own_rows(hit)
    other = own_rows(other)
    rank = jnp.zeros_like(hit)
    for d in range(1, 4):
        rank = rank + jnp.where(lane % 4 >= d, pltpu.roll(hit, d, 1), 0.0)
    srow, slane = iota((128, 256), 0), iota((128, 256), 1)
    fits = (srow // 64 == (slane // 4) % 2) & ((srow % 64) // 2 == slane // 8)
    sels, spreads = [], []
    for u in range(2):
        cols = slice(256 * u, 256 * (u + 1))
        sel = jnp.where(
            fits & (rank[:, cols] == (srow % 2).astype(F32)), jnp.broadcast_to(hit[:, cols], (128, 256)), 0.0
        )
        sels.append(sel.astype(BF16))
        spreads.append(jnp.transpose(sel).astype(BF16))
    other_t = jnp.transpose(jnp.broadcast_to(other, (128, 512)))
    wl = iota((512, 128), 1)
    pick = jnp.where(wl == 96 + expert, 1.0, 0.0) - jnp.where(wl == 96 + other_t.astype(jnp.int32), 1.0, 0.0)
    e_row, e_col = iota((128, 512), 0), iota((128, 512), 1)
    spread_e = jnp.where((e_row // 16 == e_col // 128) & (e_row % 16 == e_col % 16), 1.0, 0.0).astype(BF16)
    m_row, m_col = iota((512, 512), 0), iota((512, 512), 1)
    in_place = (m_row // 8) % 8 == (m_col // 16) % 8
    s_row, s_col = iota((32, 512), 0), iota((32, 512), 1)
    fold = jnp.where((s_col // 64 == s_row % 8) & (s_col % 8 == s_row // 8), 1.0, 0.0).astype(BF16)

    for i in range(4):
        c_wp[i].wait()
        take(wp.at[i, 0], pw_r.at[i])
    w64 = wp.reshape(64, 2048)
    w128 = jnp.concatenate([w64[:, :HALF], w64[:, HALF:]], axis=0)
    for part in range(3):
        ag_take(wm, wtail, part, 1, wm_r)
    for part in range(3):
        ag_take(tb, (), part, 2, tk_r)
    for part in range(3):
        ag_send(wm, wtail, part, 2, wm_s, wm_r)
    proj = dot_nt(tb.reshape(512, HALF)[...], w128)
    proj = proj + pltpu.roll(pltpu.roll(proj, 508, 0), 64, 1)
    msg.reshape(512, 128)[...] = proj.astype(BF16)

    @pl.loop(1, 64)
    def _(j):
        to = (chip + j) % 64
        remote(msg.at[to], rcv.at[chip], a2_s, a2_r, 2 * to + core)

    rcv[chip] = msg[chip]

    wd[...] = jnp.zeros_like(wd)
    wdd[...] = jnp.zeros_like(wdd)
    for i in range(6):
        c_w[i].wait()
    for i, b in enumerate((dg, du, dd, eg, eu, ed)):
        take(b.at[0], pw_r.at[4 + i])
    for c in range(2):
        for h in range(2):
            ls = slice(HALF * h, HALF * (h + 1))
            wd[256 * h + 48 * c : 256 * h + 48 * c + 44, :] = dg[c, :, ls]
            wd[256 * h + 128 + 48 * c : 256 * h + 128 + 48 * c + 44, :] = du[c, :, ls]
            wdd[128 * h + 48 * c : 128 * h + 48 * c + 44, :] = dd[c, :, ls]
    for h in range(2):
        ls = slice(HALF * h, HALF * (h + 1))
        wd[256 * h + 96 : 256 * h + 104, :] = rt[:, ls]
        wd[256 * h + 104 : 256 * h + 105, :] = br[:, ls]

    take(rcv.at[0:63], a2_r)
    wide = dot(rcv.reshape(512, 128)[...], spread_e)
    wide = jnp.where(in_place, wide, 0.0).astype(BF16)
    rows = dot(fold, wide)
    query, f_in, value, outgate = (rows[:, 128 * i : 128 * (i + 1)] for i in range(4))
    low = jnp.concatenate([lb[...]] * 4, axis=0)
    forget = low + (1.0 - low) * sigmoid(f_in)
    keyed = (1.0 - low) * sigmoid(-f_in)
    cols = jnp.transpose(jnp.concatenate([forget, keyed, query, query], axis=0))
    c_out = []
    for t in range(4):
        c_st[t].wait()
        for h in range(8):
            r = 8 * t + h
            fresh = cols[:, r : r + 1] * st[t, h] + cols[:, 32 + r : 33 + r] * value[r : r + 1, :]
            nst[t, h] = fresh
            rd[r : r + 1, :] = jnp.sum(fresh * cols[:, 64 + r : 65 + r], axis=0, keepdims=True)
        c_out.append(local(nst.at[t], nst_h.at[t], nsem.at[t]))
    read = rd[...]
    scaled = read * lax.rsqrt(jnp.mean(read * read, axis=1, keepdims=True) + HEAD_EPS) * hg[...]
    mixed = (scaled * (outgate * sigmoid(outgate))).astype(BF16).astype(F32)
    spread_m = jnp.where(
        iota((32, HALF), 0) % 8 == iota((32, HALF), 1) // 128, jnp.concatenate([mixed] * 8, axis=1), 0.0
    ).astype(BF16)
    for part in range(3):
        ag_take(wm, wtail, part, 2, wm_r)
    remote(
        wm.at[:, :, :, core], wm.at[:, :, :, core], wmx_s, wmx_r, partner
    )
    take(wm.at[:, :, :, 0], wmx_r)
    mo = dot_nt(spread_m, wm.reshape(2048, HALF)[...])
    mo = jnp.sum(mo.reshape(4, 8, 2048), axis=1).astype(BF16).astype(F32)
    pre = ALPHA * toks + mo
    center = jnp.mean(pre, axis=1, keepdims=True)
    var = jnp.mean(jnp.square(pre - center), axis=1, keepdims=True)
    normed = ((pre - center) * lax.rsqrt(var + NORM_EPS) * g1[...] + b1[...]).astype(BF16).astype(F32)
    nblk = jnp.concatenate([normed[:, :HALF], normed[:, HALF:]], axis=0)
    nb[own] = nblk.astype(BF16)

    for phase in range(3):
        for part in range(3):
            if phase:
                ag_take(nb, (), part, phase - 1, nb_r)
            ag_send(nb, (), part, phase, nb_s, nb_r)
    for part in range(3):
        ag_take(nb, (), part, 2, nb_r)

    nbv = nb.reshape(512, HALF)
    for u in range(2):
        sel = dot(sels[u], nbv[256 * u : 256 * (u + 1), :]).astype(BF16)
        xe[64 * u : 64 * (u + 1), :HALF] = sel[:64]
        xe[64 * u : 64 * (u + 1), HALF:] = sel[64:]
    gate = dot_nt(xe[...], eg.reshape(896, 2048)[...])
    up = dot_nt(xe[...], eu.reshape(896, 2048)[...])
    hidden = (gate * sigmoid(gate) * up).astype(BF16)
    y2 = dot_nt(nbv[...], wd[...])
    first_half = (iota((512, 256), 0) // 4) % 2 == 0
    y = jnp.where(first_half, y2[:, :256], y2[:, 256:]).reshape(64, 8, 256)
    y = (y + pltpu.roll(y, 4, 1)).reshape(512, 256)
    yg = y[:, :128]
    weight = sigmoid(jnp.sum(yg * pick, axis=1, keepdims=True))
    branch = sigmoid(yg[:, 104:105])
    hd = yg * sigmoid(yg) * y[:, 128:] * branch
    top = (iota((512, 128), 0) // 4) % 2 == 0
    hdd = jnp.concatenate([jnp.where(top, hd, 0.0), jnp.where(top, 0.0, hd)], axis=1).astype(BF16)
    slots = dot(hidden, ed.reshape(896, 2048)[...]).astype(BF16)
    obv = ob.reshape(512, HALF)
    for u in range(2):
        ru = slice(256 * u, 256 * (u + 1))
        rows_u = jnp.concatenate([slots[64 * u : 64 * (u + 1), :HALF], slots[64 * u : 64 * (u + 1), HALF:]], axis=0)
        total = weight[ru] * dot(spreads[u], rows_u) + dot(hdd[ru], wdd[...])
        obv[ru, :] = total.astype(BF16)

    r1s, r2s, r3s = (r1a, r1b, r1c), (r2a, r2b, r2c), (r3a, r3b, r3c)
    t1s, t2s = (t1a, t1b, t1c), (t2a, t2b, t2c)

    def rs_send(src, axis, rank_of, dst, dim, part, phase):
        for k in (2, 1, 3):
            c = (at[dim] + k) % 4
            idx = [slice(None)] * rank_of
            idx[axis] = c
            remote(src.at[tuple(idx)], dst.at[k - 1], rs_s.at[part, phase], rs_r.at[part, phase], peer(dim, k))

    for part in range(3):
        lanes, order = PARTS[part]
        rs_send(ob.at[:, :, :, :, lanes], order[0], 3, r1s[part], order[0], part, 0)
    for part in range(3):
        lanes, order = PARTS[part]
        d1, d2, _ = order
        take(r1s[part], rs_r.at[part, 0])
        idx = tuple(at[d] if d == d1 else slice(None) for d in range(3))
        total = ob[idx + (slice(None), lanes)].astype(F32)
        for k in range(3):
            total = total + r1s[part][k].astype(F32)
        t1s[part][...] = total.astype(BF16)
        axis = [d for d in range(3) if d != d1].index(d2)
        rs_send(t1s[part], axis, 2, r2s[part], d2, part, 1)
    for part in range(3):
        d1, d2, d3 = PARTS[part][1]
        take(r2s[part], rs_r.at[part, 1])
        axis = [d for d in range(3) if d != d1].index(d2)
        idx = [slice(None)] * 2
        idx[axis] = at[d2]
        total = t1s[part][tuple(idx)].astype(F32)
        for k in range(3):
            total = total + r2s[part][k].astype(F32)
        t2s[part][...] = total.astype(BF16)
        rs_send(t2s[part], 0, 1, r3s[part], d3, part, 2)
    chans = []
    for part in range(3):
        d3 = PARTS[part][1][2]
        take(r3s[part], rs_r.at[part, 2])
        total = t2s[part][at[d3]].astype(F32)
        for k in range(3):
            total = total + r3s[part][k].astype(F32)
        chans.append(total)
    z = ALPHA * nblk + jnp.concatenate(chans, axis=1)

    def both(v):
        v = jnp.broadcast_to(v, (8, 128))
        return (v + pltpu.roll(v, 4, 0))[:, 0:1]

    def by_half(ref):
        v = ref[...]
        return jnp.concatenate(
            [jnp.broadcast_to(v[:, :HALF], (4, HALF)), jnp.broadcast_to(v[:, HALF:], (4, HALF))], axis=0
        )

    center = both(jnp.sum(z, axis=1, keepdims=True)) * (1.0 / 2048)
    dev = z - center
    var = both(jnp.sum(dev * dev, axis=1, keepdims=True)) * (1.0 / 2048)
    res = dev * lax.rsqrt(var + NORM_EPS) * by_half(g2) + by_half(b2)
    out_ref[:, :HALF] = res[:4].astype(BF16)
    out_ref[:, HALF:] = res[4:].astype(BF16)

    for c in c_out:
        c.wait()
    for i in range(4):
        take(wp.at[i, 0], pw_s.at[i])
    for i, b in enumerate((dg, du, dd, eg, eu, ed)):
        take(b.at[0], pw_s.at[4 + i])
    take(wm.at[:, :, :, 0], wmx_s)
    take(msg.at[0:63], a2_s)
    for part in range(3):
        for phase in range(3):
            take(three(tb, (), part, phase), tk_s.at[part, phase])
            take(three(nb, (), part, phase), nb_s.at[part, phase])
            take(three(wm, (0,), part, phase), wm_s.at[part, phase])
        take(r1s[part], rs_s.at[part, 0])
        take(r2s[part], rs_s.at[part, 1])
        take(r3s[part], rs_s.at[part, 2])


def per_device(
    tokens, recurrent_state, query_weight, forget_weight, input_weight, outgate_weight, lower_bound, head_gain,
    mixout_weight, first_gain, first_bias, router_weight, branch_vector, dense_gate_weight, dense_up_weight,
    dense_down_weight, expert_gate_weight, expert_up_weight, expert_down_weight, second_gain, second_bias, routes,
):
    args = (
        tokens, recurrent_state, query_weight.T, forget_weight.T, input_weight.T, outgate_weight.T,
        lower_bound.reshape(8, 128), head_gain.reshape(1, 128), mixout_weight.T, first_gain.reshape(1, 2048),
        first_bias.reshape(1, 2048), router_weight.T, branch_vector.reshape(1, 2048), dense_gate_weight.T,
        dense_up_weight.T, dense_down_weight, expert_gate_weight.T, expert_up_weight.T, expert_down_weight,
        second_gain.reshape(1, 2048), second_bias.reshape(1, 2048), routes.T,
    )
    lanes = [p[0].stop - p[0].start for p in PARTS]
    V = pltpu.VMEM
    sem = pltpu.SemaphoreType.DMA
    scratch = [
        V((4, 2048), BF16), V((4, 8, 128, 128), F32), V((4, 8, 128, 128), F32), V((4, 2, 8, 2048), BF16),
        V((8, 128), F32), V((1, 128), F32), V((4, 4, 4, 2, 16, HALF), BF16), V((1, 2048), F32), V((1, 2048), F32),
        V((8, 2048), BF16), V((1, 2048), BF16), V((2, 44, 2048), BF16), V((2, 44, 2048), BF16),
        V((2, 44, 2048), BF16), V((2, 448, 2048), BF16), V((2, 448, 2048), BF16), V((2, 448, 2048), BF16),
        V((1, 2048), F32), V((1, 2048), F32), V((2, 512), jnp.int32),
        V((4, 4, 4, 8, HALF), BF16), V((4, 4, 4, 8, HALF), BF16), V((64, 8, 128), BF16), V((64, 8, 128), BF16),
        V((4, 4, 4, 8, HALF), BF16), V((128, 2048), BF16), V((512, HALF), BF16), V((256, HALF), BF16),
        V((32, 128), F32),
        *[V((3, 4, 4, 8, n), BF16) for n in lanes], *[V((3, 4, 8, n), BF16) for n in lanes],
        *[V((3, 8, n), BF16) for n in lanes], *[V((4, 4, 8, n), BF16) for n in lanes],
        *[V((4, 8, n), BF16) for n in lanes],
        sem((21,)), sem((4,)), sem((4,)), sem((10,)), sem((10,)), sem((3, 3)), sem((3, 3)), sem(()), sem(()),
        sem((3, 3)), sem((3, 3)), sem((3, 3)), sem((3, 3)), sem(()), sem(()), sem((3, 3)), sem((3, 3)),
    ]
    hbm = pl.BlockSpec(memory_space=pl.ANY)
    return pl.pallas_call(
        kernel,
        out_shape=(jax.ShapeDtypeStruct((4, 2048), BF16), jax.ShapeDtypeStruct((4, 8, 128, 128), F32)),
        in_specs=[hbm] * 22,
        out_specs=(pl.BlockSpec(memory_space=pltpu.VMEM), hbm),
        scratch_shapes=scratch,
        compiler_params=pltpu.CompilerParams(
            collective_id=0, has_side_effects=True, vmem_limit_bytes=60 * 1024 * 1024
        ),
        name="layer",
    )(*args)


def solution(mesh):
    ep = "ep"
    cols, rows = P(None, ep), P(ep, None)
    return jax.shard_map(
        per_device,
        mesh=mesh,
        in_specs=(
            rows, P(ep, None, None, None), cols, cols, cols, cols, P(), P(), cols, P(), P(), P(), P(),
            cols, cols, rows, cols, cols, rows, P(), P(), P(),
        ),
        out_specs=(rows, P(ep, None, None, None)),
        check_vma=False,
    )
```

time: 231 us -> 80.6 us (0.35)
  blocking collectives: 108 us -> 0 us
  Pallas kernels: 0 us -> 73.9 us
  local copies, waits for them, and re-layouts: 41.3 us -> 5.76 us
  matrix products: 33.5 us -> 0 us
  waiting for transfers between devices: 27.8 us -> 0 us
  starting transfers between devices: 9.75 us -> 0 us
  other arithmetic: 8.75 us -> 0 us
    all_to_all x8 -> x0, blocking collectives: 108 us -> none  [the longest x5 64.1 us: from_everyone(): lax.all_to_all(jnp.broadcast_to(shard[None], (devices, *shard.shape)), ax...]
    pallas_call x0 -> x1, Pallas kernels: none -> 73.9 us  [per_device(): pl.pallas_call(kernel, out_shape=(jax.ShapeDtypeStruct((4, 2048), BF16),...]
    dot_general x11 -> x0, matrix products: 33.5 us -> none  [the longest x1 7.84 us: channel_term(): jnp.einsum('sci,scd->sid', select.astype(f32), slot_out, precision=lax.Pr...]
    all_to_all x2 -> x0, waiting for transfers between devices: 27.8 us -> none  [the longest x1 18.5 us: from_everyone(): lax.all_to_all(jnp.broadcast_to(shard[None], (devices, *shard.shape)), ax...]
    another operation x5 -> x0, local copies, waits for them, and re-layouts: 16 us -> none  [the longest x3 9.11 us: laid_out(): return jnp.moveaxis(parts, 0, dim).reshape(dims)]
    all_to_all x2 -> x0, starting transfers between devices: 9.75 us -> none  [the longest x1 5.14 us: from_everyone(): lax.all_to_all(jnp.broadcast_to(shard[None], (devices, *shard.shape)), ax...]
    reshape x4 -> x1, local copies, waits for them, and re-layouts: 10.9 us -> 1.29 us  [per_device(): branch_vector.reshape(1, 2048)]
    transpose x4 -> x0, local copies, waits for them, and re-layouts: 6.34 us -> none  [the longest x3 6.06 us: gathered_by_axis(): parts = jnp.swapaxes(from_everyone(leading, near), 0, 1)]
  transfers between devices with their start and end apart: 2 -> 0, of which waited for: 2 -> 0; matrix products, arithmetic and copies ran while one was open for 0% -> 0% of each run, Pallas kernels for 0% -> 0%
where the time goes in v1:
time: 80.6 us; the launch traced here: 80.3 us
  Pallas kernels  73.9 us (92%)
  local copies, waits for them, and re-layouts  5.76 us (7%)
    pallas_call x1, Pallas kernels, per_device(): pl.pallas_call(kernel, out_shape=(jax.ShapeDtypeStruct((4, 2048), BF16),...  73.9 us
    unnamed x2, local copies, waits for them, and re-layouts  4.46 us

profile of v1, /device:TPU:0, one launch (start us, length us, event | category | flops | bytes accessed | tf_op | source)
XLA Modules:
  0.0 80.3 jit_solution(18306527076253721876)
XLA Ops:
  0.6 1.3 %reshape.29.branch_h = bf16[1,2048]{1,0:T(2,128)(2,1)} reshape(bf16[2048]{0:T(1024)(128)(2,1)} %param.34) | data formatting | bytes 8192 | tf_op jit(solution)/shard_map/reshape | solution.py:374
  1.9 73.9 %layer.1 = (bf16[4,2048]{1,0:T(4,128)(2,1)}, f32[4,8,128,128]{3,2,1,0:T(8,128)}) custom-call(bf16[4,2048]{1,0:T(4,128)(2,1)} %tok_h.1, f32[4,8,128,128]{3,2,1,0:T(8,128)} %state_h.1, bf16[8,2048]{1,0:T(8,128)(2,1)} %bitcast.21, bf16[8,2048]{1,0:T(8,128)(2,1)} %bitcast.22, bf16[8,2048]{1,0:T(8,128)(2,1)} %bitcast.23, bf16[8,2048]{1,0:T(8,128)(2,1)} %bitcast.24, ...), custom_call_target="tpu_custom_call" | custom-call | tf_op jit(solution)/shard_map/layer/pallas_call | solution.py:397
  75.8 1.3 %copy.26 = bf16[4,2048]{1,0:T(4,128)(2,1)} copy(bf16[4,2048]{1,0:T(4,128)(2,1)} %get-tuple-element.4) | data formatting | bytes 32768
  77.2 3.1 %copy.27 = f32[4,8,128,128]{3,2,1,0:T(8,128)} copy(f32[4,8,128,128]{3,2,1,0:T(8,128)} %get-tuple-element.5) | data formatting | bytes 4194304

commit v2 on v1

v2 whole, which is shorter than its diff:
```python
import functools

import jax
import jax.numpy as jnp
from jax import lax
from jax.experimental import pallas as pl
from jax.experimental.pallas import tpu as pltpu
from jax.sharding import PartitionSpec as P

ALPHA = 8.0**0.25
NORM_EPS = 1e-05
HEAD_EPS = 1e-06
HALF = 1024
F32 = jnp.float32
BF16 = jnp.bfloat16
ALL = slice(None)
ORDERS = ((2, 1, 0), (1, 0, 2), (0, 2, 1))
LANES = (slice(0, 384), slice(384, 768), slice(768, 1024))
TAILS = tuple((ALL, lanes) for lanes in LANES)
WTAILS = ((ALL, slice(0, 8), slice(0, 384)), (ALL, slice(8, 16), slice(0, 384)), (ALL, ALL, slice(384, 512)))
NT = (((1,), (1,)), ((), ()))


def dot(a, b):
    return jnp.dot(a, b, preferred_element_type=F32)


def dot_nt(a, b):
    return lax.dot_general(a, b, NT, preferred_element_type=F32)


def iota(shape, dim):
    return lax.broadcasted_iota(jnp.int32, shape, dim)


def id_of(part):
    return part if isinstance(part, int) else id(part)


def sigmoid(a):
    return 1.0 / (1.0 + jnp.exp(-a))


def kernel(
    tok_h, state_h, wq_h, wf_h, wi_h, wo_h, lb_h, hg_h, wm_h, g1_h, b1_h, router_h, branch_h,
    dg_h, du_h, dd_h, eg_h, eu_h, ed_h, g2_h, b2_h, routes_h,
    out_h, nst_h,
    tokv, outv, st, nst, wp, lb, hg, wm, g1, b1, rt, br, dg, du, dd, eg, eu, ed, g2, b2, rts,
    tb, nb, msg, rcv, ob, xe, wd, wdd, rd,
    r1a, r1b, r1c, r2a, r2b, r2c, t1a, t1b, t1c, mx, mos, mor,
    loc, stsem, nsem, pw_s, pw_r, wm_s, wm_r, wmx_s, wmx_r, mx_s, mx_r, tk_s, tk_r, nb_s, nb_r, a2_s, a2_r, rs_s, rs_r,
):
    me = lax.axis_index("ep")
    core = me % 2
    chip = me // 2
    at = (chip // 16, (chip // 4) % 4, chip % 4)
    partner = me + 1 - 2 * core

    def peer(steps):
        c = [(at[d] + steps[d]) % 4 if steps.get(d) else at[d] for d in range(3)]
        return 2 * ((c[0] * 4 + c[1]) * 4 + c[2]) + core

    def remote(src, dst, ss, rs, dev):
        pltpu.make_async_remote_copy(
            src_ref=src, dst_ref=dst, send_sem=ss, recv_sem=rs, device_id=(dev,),
            device_id_type=pl.DeviceIdType.MESH,
        ).start()

    sent, due = {}, {}

    def local(src, dst, sem):
        cp = pltpu.make_async_copy(src, dst, sem)
        cp.start()
        return cp

    def expect(key, ref, ss, rs):
        key = tuple(map(id_of, key)) if isinstance(key, tuple) else id_of(key)
        sent[key] = functools.partial(take, ref, ss)
        due[key] = functools.partial(take, ref, rs)

    def got(key):
        key = tuple(map(id_of, key)) if isinstance(key, tuple) else id_of(key)
        due.pop(key)()

    def take(ref, sem):
        pltpu.make_async_copy(ref, ref, sem).wait()

    own = (at[0], at[1], at[2])
    c_tok = local(tok_h, tokv, loc.at[0])
    c_wp = [local(w, wp.at[i, core], loc.at[1 + i]) for i, w in enumerate((wq_h, wf_h, wi_h, wo_h))]
    half_own = pl.ds(pl.multiple_of(core * 512, 512), 512)
    c_wm = local(wm_h.at[:, half_own], wm.at[own + (core,)], loc.at[5])
    c_small = [
        local(a, b, loc.at[6 + i])
        for i, (a, b) in enumerate(
            ((lb_h, lb), (hg_h, hg), (g1_h, g1), (b1_h, b1), (router_h, rt), (branch_h, br),
             (g2_h, g2), (b2_h, b2), (routes_h, rts))
        )
    ]
    barrier = pltpu.get_barrier_semaphore()
    steps = [{d1: k1, d2: k2} for d1, d2 in ((0, 1), (0, 2), (1, 2)) for k1 in (2, 1, 3) for k2 in (2, 1, 3)]
    steps += [{d: k} for d in range(3) for k in (2, 1, 3)]
    for step in steps:
        pl.semaphore_signal(barrier, inc=1, device_id=(peer(step),), device_id_type=pl.DeviceIdType.MESH)
    pl.semaphore_signal(barrier, inc=1, device_id=(partner,), device_id_type=pl.DeviceIdType.MESH)
    c_tok.wait()
    toks = tokv[...].astype(F32)
    tblk = jnp.concatenate([toks[:, :HALF], toks[:, HALF:]], axis=0).astype(BF16)
    tb[own] = tblk
    pl.semaphore_wait(barrier, 37)

    def region(part, fixed):
        return tuple(fixed.get(d, ALL) for d in range(3))

    def blocks(buf, tail, count):
        idx = {3: (0, 0, slice(0, 3)), 4: (0, 0, ALL), 12: (0, slice(0, 3), ALL), 48: (slice(0, 3), ALL, ALL)}[count]
        return buf.at[idx + tail]

    def plane_send(buf, part, ss, rs):
        d1, d2, _ = ORDERS[part]
        ref = buf.at[own + TAILS[part]]
        for k2 in (2, 1, 3, 0):
            for k1 in (2, 1, 3, 0):
                if k1 or k2:
                    remote(ref, ref, ss.at[part, k2], rs.at[part, (4 - k2) % 4], peer({d1: k1, d2: k2}))
        for g in range(4):
            expect((ss, part, g), blocks(buf, TAILS[part], 4 if g else 3), ss.at[part, g], rs.at[part, g])

    def line_send(buf, part, g, ss, rs):
        d1, d2, d3 = ORDERS[part]
        got((ss, part, g))
        idx = region(part, {d2: (at[d2] + g) % 4, d3: at[d3]})
        ref = buf.at[idx + TAILS[part]]
        for k in (2, 1, 3):
            remote(ref, ref, ss.at[part, 4], rs.at[part, 4], peer({d3: k}))
        if g == 2:
            expect((ss, part, 4), blocks(buf, TAILS[part], 48), ss.at[part, 4], rs.at[part, 4])

    def walk_send(buf, part, phase, ss, rs):
        order = ORDERS[part]
        if phase:
            got((ss, part, phase - 1))
        idx = region(part, {d: at[d] for d in order[phase:]})
        ref = buf.at[idx + WTAILS[part]]
        for k in (2, 1, 3):
            remote(ref, ref, ss.at[part, phase], rs.at[part, phase], peer({order[phase]: k}))
        expect((ss, part, phase), blocks(buf, WTAILS[part], (3, 12, 48)[phase]), ss.at[part, phase], rs.at[part, phase])

    for part in range(3):
        plane_send(tb, part, tk_s, tk_r)
    half_in = pl.ds(pl.multiple_of((1 - core) * 512, 512), 512)
    remote(wm_h.at[:, half_in], wm.at[own + (core,)], wmx_s, wmx_r, partner)
    expect(wmx_s, wm.at[own + (0,)], wmx_s, wmx_r)
    for i, w in enumerate((wq_h, wf_h, wi_h, wo_h)):
        remote(w, wp.at[i, core], pw_s.at[i], pw_r.at[i], partner)
        expect((pw_s, i), wp.at[i, 0], pw_s.at[i], pw_r.at[i])
    c_st = [local(state_h.at[t], st.at[t], stsem.at[t]) for t in range(4)]
    c_w = []
    big = ((dg_h, dg), (du_h, du), (dd_h, dd), (eg_h, eg), (eu_h, eu), (ed_h, ed))
    for i, (a, b) in enumerate(big):
        c_w.append(local(a, b.at[core], loc.at[15 + i]))
    for g in (0, 1, 3, 2):
        for part in range(3):
            line_send(tb, part, g, tk_s, tk_r)
    c_wm.wait()
    got(wmx_s)
    for part in range(3):
        walk_send(wm, part, 0, wm_s, wm_r)
    for i, (a, b) in enumerate(big):
        remote(a, b.at[core], pw_s.at[4 + i], pw_r.at[4 + i], partner)
        expect((pw_s, 4 + i), b.at[0], pw_s.at[4 + i], pw_r.at[4 + i])

    for c in c_small:
        c.wait()
    expert = chip // 8
    r0 = rts[0:1, :]
    r1 = rts[1:2, :]
    lane = iota((1, 512), 1)
    hit = jnp.where((r0 == expert) | (r1 == expert), 1.0, 0.0)
    other = jnp.where(r0 == expert, r1, r0).astype(F32)
    mine = (lane // 4) % 2 == core

    def own_rows(v):
        moved = jnp.where(core == 0, pltpu.roll(v, 4, 1), pltpu.roll(v, 508, 1))
        return jnp.where(mine, v, moved)

    hit = own_rows(hit)
    other = own_rows(other)
    rank = jnp.zeros_like(hit)
    for d in range(1, 4):
        rank = rank + jnp.where(lane % 4 >= d, pltpu.roll(hit, d, 1), 0.0)
    srow, slane = iota((128, 256), 0), iota((128, 256), 1)
    fits = (srow // 64 == (slane // 4) % 2) & ((srow % 64) // 2 == slane // 8)
    sels, spreads = [], []
    for u in range(2):
        cols = slice(256 * u, 256 * (u + 1))
        sel = jnp.where(
            fits & (rank[:, cols] == (srow % 2).astype(F32)), jnp.broadcast_to(hit[:, cols], (128, 256)), 0.0
        )
        sels.append(sel.astype(BF16))
        spreads.append(jnp.transpose(sel).astype(BF16))
    other_t = jnp.transpose(jnp.broadcast_to(other, (128, 512)))
    wl = iota((512, 128), 1)
    pick = jnp.where(wl == 96 + expert, 1.0, 0.0) - jnp.where(wl == 96 + other_t.astype(jnp.int32), 1.0, 0.0)
    e_row, e_col = iota((128, 512), 0), iota((128, 512), 1)
    spread_e = jnp.where((e_row // 16 == e_col // 128) & (e_row % 16 == e_col % 16), 1.0, 0.0).astype(BF16)
    m_row, m_col = iota((512, 512), 0), iota((512, 512), 1)
    in_place = (m_row // 8) % 8 == (m_col // 16) % 8
    s_row, s_col = iota((32, 512), 0), iota((32, 512), 1)
    fold = jnp.where((s_col // 64 == s_row % 8) & (s_col % 8 == s_row // 8), 1.0, 0.0).astype(BF16)

    for i in range(4):
        c_wp[i].wait()
        got((pw_s, i))
    w64 = wp.reshape(64, 2048)
    w128 = jnp.concatenate([w64[:, :HALF], w64[:, HALF:]], axis=0)
    for part in range(3):
        walk_send(wm, part, 1, wm_s, wm_r)
    for part in range(3):
        got((tk_s, part, 4))
    proj = dot_nt(tb.reshape(512, HALF)[...], w128)
    proj = proj + pltpu.roll(pltpu.roll(proj, 508, 0), 64, 1)
    msg.reshape(512, 128)[...] = proj.astype(BF16)

    @pl.loop(1, 64)
    def _(j):
        to = (chip + j) % 64
        remote(msg.at[to], rcv.at[chip], a2_s, a2_r, 2 * to + core)

    expect(a2_s, rcv.at[0:63], a2_s, a2_r)
    rcv[chip] = msg[chip]
    for part in range(3):
        walk_send(wm, part, 2, wm_s, wm_r)

    wd[...] = jnp.zeros_like(wd)
    wdd[...] = jnp.zeros_like(wdd)
    for i in range(6):
        c_w[i].wait()
        got((pw_s, 4 + i))
    for c in range(2):
        for h in range(2):
            ls = slice(HALF * h, HALF * (h + 1))
            wd[256 * h + 48 * c : 256 * h + 48 * c + 44, :] = dg[c, :, ls]
            wd[256 * h + 128 + 48 * c : 256 * h + 128 + 48 * c + 44, :] = du[c, :, ls]
            wdd[128 * h + 48 * c : 128 * h + 48 * c + 44, :] = dd[c, :, ls]
    for h in range(2):
        ls = slice(HALF * h, HALF * (h + 1))
        brow = jnp.concatenate([br[8 * h + i : 8 * h + i + 1, :].astype(F32) for i in range(8)], axis=1)
        extra = jnp.concatenate([rt[:, ls].astype(F32), brow, jnp.zeros((7, HALF), F32)], axis=0)
        wd[256 * h + 96 : 256 * h + 112, :] = extra.astype(BF16)

    got(a2_s)
    wide = dot(rcv.reshape(512, 128)[...], spread_e)
    wide = jnp.where(in_place, wide, 0.0).astype(BF16)
    rows = dot(fold, wide)
    query, f_in, value, outgate = (rows[:, 128 * i : 128 * (i + 1)] for i in range(4))
    low = jnp.concatenate([lb[...]] * 4, axis=0)
    forget = low + (1.0 - low) * sigmoid(f_in)
    keyed = (1.0 - low) * sigmoid(-f_in)
    cols = jnp.transpose(jnp.concatenate([forget, keyed, query, query], axis=0))
    c_out = []
    for t in range(4):
        c_st[t].wait()
        for h in range(8):
            r = 8 * t + h
            fresh = cols[:, r : r + 1] * st[t, h] + cols[:, 32 + r : 33 + r] * value[r : r + 1, :]
            nst[t, h] = fresh
            rd[r : r + 1, :] = jnp.sum(fresh * cols[:, 64 + r : 65 + r], axis=0, keepdims=True)
        c_out.append(local(nst.at[t], nst_h.at[t], nsem.at[t]))
    read = rd[...]
    scaled = read * lax.rsqrt(jnp.mean(read * read, axis=1, keepdims=True) + HEAD_EPS) * hg[...]
    mx[core] = (scaled * (outgate * sigmoid(outgate))).astype(BF16).astype(F32)
    remote(mx.at[core], mx.at[core], mx_s.at[0], mx_r.at[0], partner)
    expect((mx_s, 0), mx.at[0], mx_s.at[0], mx_r.at[0])
    for part in range(3):
        got((wm_s, part, 2))
    got((mx_s, 0))
    mxv = mx.reshape(64, 128)
    lhs = jnp.concatenate([mxv[pl.ds(4 * core + i, 8, stride=8), :] for i in range(4)], axis=1).astype(BF16)
    mo = dot_nt(lhs, wm.reshape(2048, 512)[...])
    mos[0] = mo[:4]
    mos[1] = mo[4:]
    remote(mos.at[1 - core], mor, mx_s.at[1], mx_r.at[1], partner)
    expect((mx_s, 1), mor, mx_s.at[1], mx_r.at[1])
    mo = mos[core]
    got((mx_s, 1))
    mo = (mo + mor[...]).astype(BF16).astype(F32)
    pre = ALPHA * toks + mo
    center = jnp.mean(pre, axis=1, keepdims=True)
    var = jnp.mean(jnp.square(pre - center), axis=1, keepdims=True)
    normed = ((pre - center) * lax.rsqrt(var + NORM_EPS) * g1[...] + b1[...]).astype(BF16).astype(F32)
    nblk = jnp.concatenate([normed[:, :HALF], normed[:, HALF:]], axis=0)
    nb[own] = nblk.astype(BF16)

    for part in range(3):
        plane_send(nb, part, nb_s, nb_r)
    for g in (0, 1, 3, 2):
        for part in range(3):
            line_send(nb, part, g, nb_s, nb_r)
    for part in range(3):
        got((nb_s, part, 4))

    nbv = nb.reshape(512, HALF)
    for u in range(2):
        sel = dot(sels[u], nbv[256 * u : 256 * (u + 1), :]).astype(BF16)
        xe[64 * u : 64 * (u + 1), :HALF] = sel[:64]
        xe[64 * u : 64 * (u + 1), HALF:] = sel[64:]
    gate = dot_nt(xe[...], eg.reshape(896, 2048)[...])
    up = dot_nt(xe[...], eu.reshape(896, 2048)[...])
    hidden = (gate * sigmoid(gate) * up).astype(BF16)
    y2 = dot_nt(nbv[...], wd[...])
    first_half = (iota((512, 256), 0) // 4) % 2 == 0
    y = jnp.where(first_half, y2[:, :256], y2[:, 256:]).reshape(64, 8, 256)
    y = (y + pltpu.roll(y, 4, 1)).reshape(512, 256)
    yg = y[:, :128]
    weight = sigmoid(jnp.sum(yg * pick, axis=1, keepdims=True))
    branch = sigmoid(yg[:, 104:105])
    hd = yg * sigmoid(yg) * y[:, 128:] * branch
    top = (iota((512, 128), 0) // 4) % 2 == 0
    hdd = jnp.concatenate([jnp.where(top, hd, 0.0), jnp.where(top, 0.0, hd)], axis=1).astype(BF16)
    slots = dot(hidden, ed.reshape(896, 2048)[...]).astype(BF16)
    obv = ob.reshape(512, HALF)
    for u in range(2):
        ru = slice(256 * u, 256 * (u + 1))
        rows_u = jnp.concatenate([slots[64 * u : 64 * (u + 1), :HALF], slots[64 * u : 64 * (u + 1), HALF:]], axis=0)
        total = weight[ru] * dot(spreads[u], rows_u) + dot(hdd[ru], wdd[...])
        obv[ru, :] = total.astype(BF16)

    r1s, r2s, t1s = (r1a, r1b, r1c), (r2a, r2b, r2c), (t1a, t1b, t1c)
    spots = ((2, 0), (1, 1), (3, 2), (0, 3))
    for g, slot in spots:
        for part in range(3):
            d1, d2, _ = ORDERS[part]
            for k in (2, 1, 3):
                idx = region(part, {d1: (at[d1] + k) % 4, d2: (at[d2] + g) % 4})
                remote(
                    ob.at[idx + TAILS[part]], r1s[part].at[slot, k - 1], rs_s.at[part, slot], rs_r.at[part, slot],
                    peer({d1: k}),
                )
            expect((rs_s, part, slot), r1s[part].at[slot], rs_s.at[part, slot], rs_r.at[part, slot])
    for g, slot in spots:
        for part in range(3):
            d1, d2, d3 = ORDERS[part]
            got((rs_s, part, slot))
            idx = region(part, {d1: at[d1], d2: (at[d2] + g) % 4})
            total = ob[idx + TAILS[part]].astype(F32)
            for k in range(3):
                total = total + r1s[part][slot, k].astype(F32)
            t1s[part][slot] = total.astype(BF16)
            for k in (2, 1, 3, 0):
                if k or g:
                    remote(
                        t1s[part].at[slot, (at[d3] + k) % 4], r2s[part].at[4 * g + k - 1], rs_s.at[part, 4],
                        rs_r.at[part, 4], peer({d2: g, d3: k}),
                    )
    chans = []
    for part in range(3):
        d3 = ORDERS[part][2]
        take(r2s[part], rs_r.at[part, 4])
        total = t1s[part][3, at[d3]].astype(F32)
        for k in range(15):
            total = total + r2s[part][k].astype(F32)
        chans.append(total)
        sent[f"r{part}"] = functools.partial(take, r2s[part], rs_s.at[part, 4])
    z = ALPHA * nblk + jnp.concatenate(chans, axis=1)

    def both(v):
        v = jnp.broadcast_to(v, (8, 128))
        return (v + pltpu.roll(v, 4, 0))[:, 0:1]

    def by_half(ref):
        v = ref[...]
        return jnp.concatenate(
            [jnp.broadcast_to(v[:, :HALF], (4, HALF)), jnp.broadcast_to(v[:, HALF:], (4, HALF))], axis=0
        )

    center = both(jnp.sum(z, axis=1, keepdims=True)) * (1.0 / 2048)
    dev = z - center
    var = both(jnp.sum(dev * dev, axis=1, keepdims=True)) * (1.0 / 2048)
    res = dev * lax.rsqrt(var + NORM_EPS) * by_half(g2) + by_half(b2)
    outv[:, :HALF] = res[:4].astype(BF16)
    outv[:, HALF:] = res[4:].astype(BF16)
    c_out.append(local(outv, out_h, loc.at[0]))

    for c in c_out:
        c.wait()
    for wait in sent.values():
        wait()


def per_device(
    tokens, recurrent_state, query_weight, forget_weight, input_weight, outgate_weight, lower_bound, head_gain,
    mixout_weight, first_gain, first_bias, router_weight, branch_vector, dense_gate_weight, dense_up_weight,
    dense_down_weight, expert_gate_weight, expert_up_weight, expert_down_weight, second_gain, second_bias, routes,
):
    args = (
        tokens, recurrent_state, query_weight.T, forget_weight.T, input_weight.T, outgate_weight.T,
        lower_bound.reshape(8, 128), head_gain.reshape(1, 128), mixout_weight.T, first_gain.reshape(1, 2048),
        first_bias.reshape(1, 2048), router_weight.T, branch_vector.reshape(16, 128), dense_gate_weight.T,
        dense_up_weight.T, dense_down_weight, expert_gate_weight.T, expert_up_weight.T, expert_down_weight,
        second_gain.reshape(1, 2048), second_bias.reshape(1, 2048), routes.T,
    )
    lanes = [p.stop - p.start for p in LANES]
    V = pltpu.VMEM
    sem = pltpu.SemaphoreType.DMA
    scratch = [
        V((4, 2048), BF16), V((4, 2048), BF16), V((4, 8, 128, 128), F32), V((4, 8, 128, 128), F32), V((4, 2, 8, 2048), BF16),
        V((8, 128), F32), V((1, 128), F32), V((4, 4, 4, 2, 16, 512), BF16), V((1, 2048), F32), V((1, 2048), F32),
        V((8, 2048), BF16), V((16, 128), BF16), V((2, 44, 2048), BF16), V((2, 44, 2048), BF16),
        V((2, 44, 2048), BF16), V((2, 448, 2048), BF16), V((2, 448, 2048), BF16), V((2, 448, 2048), BF16),
        V((1, 2048), F32), V((1, 2048), F32), V((2, 512), jnp.int32),
        V((4, 4, 4, 8, HALF), BF16), V((4, 4, 4, 8, HALF), BF16), V((64, 8, 128), BF16), V((64, 8, 128), BF16),
        V((4, 4, 4, 8, HALF), BF16), V((128, 2048), BF16), V((512, HALF), BF16), V((256, HALF), BF16),
        V((32, 128), F32),
        *[V((4, 3, 4, 8, n), BF16) for n in lanes], *[V((15, 8, n), BF16) for n in lanes],
        *[V((4, 4, 8, n), BF16) for n in lanes],
        V((2, 32, 128), F32), V((2, 4, 2048), F32), V((4, 2048), F32),
        sem((21,)), sem((4,)), sem((4,)), sem((10,)), sem((10,)), sem((3, 3)), sem((3, 3)), sem(()), sem(()),
        sem((2,)), sem((2,)), sem((3, 5)), sem((3, 5)), sem((3, 5)), sem((3, 5)), sem(()), sem(()), sem((3, 5)), sem((3, 5)),
    ]
    hbm = pl.BlockSpec(memory_space=pltpu.HBM)
    free = pl.BlockSpec(memory_space=pl.ANY)
    return pl.pallas_call(
        kernel,
        out_shape=(jax.ShapeDtypeStruct((4, 2048), BF16), jax.ShapeDtypeStruct((4, 8, 128, 128), F32)),
        in_specs=[hbm] * 22,
        out_specs=(free, free),
        scratch_shapes=scratch,
        compiler_params=pltpu.CompilerParams(
            collective_id=0, has_side_effects=True, vmem_limit_bytes=60 * 1024 * 1024
        ),
        name="layer",
    )(*args)


def solution(mesh):
    ep = "ep"
    cols, rows = P(None, ep), P(ep, None)
    return jax.shard_map(
        per_device,
        mesh=mesh,
        in_specs=(
            rows, P(ep, None, None, None), cols, cols, cols, cols, P(), P(), cols, P(), P(), P(), P(),
            cols, cols, rows, cols, cols, rows, P(), P(), P(),
        ),
        out_specs=(rows, P(ep, None, None, None)),
        check_vma=False,
    )
```

time: 80.6 us -> 68.7 us (0.85)
  Pallas kernels: 73.9 us -> 63.3 us
  local copies, waits for them, and re-layouts: 5.76 us -> 4.46 us
    pallas_call x1, Pallas kernels: 73.9 us -> 63.3 us  [per_device(): pl.pallas_call(kernel, out_shape=(jax.ShapeDtypeStruct((4, 2048), BF16),...]
    reshape x1 -> x0, local copies, waits for them, and re-layouts: 1.29 us -> none  [per_device(): branch_vector.reshape(1, 2048)]
where the time goes in v2:
time: 68.7 us; the launch traced here: 68.4 us
  Pallas kernels  63.3 us (92%)
  local copies, waits for them, and re-layouts  4.46 us (6%)
    pallas_call x1, Pallas kernels, per_device(): pl.pallas_call(kernel, out_shape=(jax.ShapeDtypeStruct((4, 2048), BF16),...  63.3 us
    unnamed x2, local copies, waits for them, and re-layouts  4.46 us

profile of v2, /device:TPU:0, one launch (start us, length us, event | category | flops | bytes accessed | tf_op | source)
XLA Modules:
  0.0 68.4 jit_solution(10158931234852067242)
XLA Ops:
  0.6 63.3 %layer.1 = (bf16[4,2048]{1,0:T(4,128)(2,1)}, f32[4,8,128,128]{3,2,1,0:T(8,128)}) custom-call(bf16[4,2048]{1,0:T(4,128)(2,1)} %tok_h.1, f32[4,8,128,128]{3,2,1,0:T(8,128)} %state_h.1, bf16[8,2048]{1,0:T(8,128)(2,1)} %bitcast.22, bf16[8,2048]{1,0:T(8,128)(2,1)} %bitcast.23, bf16[8,2048]{1,0:T(8,128)(2,1)} %bitcast.24, bf16[8,2048]{1,0:T(8,128)(2,1)} %bitcast.25, ...), custom_call_target="tpu_custom_call" | custom-call | tf_op jit(solution)/shard_map/layer/pallas_call | solution.py:423
  63.9 1.3 %copy.26 = bf16[4,2048]{1,0:T(4,128)(2,1)} copy(bf16[4,2048]{1,0:T(4,128)(2,1)} %get-tuple-element.4) | data formatting | bytes 32768
  65.3 3.1 %copy.27 = f32[4,8,128,128]{3,2,1,0:T(8,128)} copy(f32[4,8,128,128]{3,2,1,0:T(8,128)} %get-tuple-element.5) | data formatting | bytes 4194304

commit v3 on v2

--- a/solution.py
+++ b/solution.py
@@ -136,15 +136,28 @@
         if g == 2:
             expect((ss, part, 4), blocks(buf, TAILS[part], 48), ss.at[part, 4], rs.at[part, 4])
 
-    def walk_send(buf, part, phase, ss, rs):
-        order = ORDERS[part]
+    def walk_send(part, phase):
+        d1, d2, d3 = ORDERS[part]
         if phase:
-            got((ss, part, phase - 1))
-        idx = region(part, {d: at[d] for d in order[phase:]})
-        ref = buf.at[idx + WTAILS[part]]
+            got((wm_s, part, 0))
+        ref = wm.at[region(part, {d: at[d] for d in (d1, d2, d3)[phase:]}) + WTAILS[part]]
         for k in (2, 1, 3):
-            remote(ref, ref, ss.at[part, phase], rs.at[part, phase], peer({order[phase]: k}))
-        expect((ss, part, phase), blocks(buf, WTAILS[part], (3, 12, 48)[phase]), ss.at[part, phase], rs.at[part, phase])
+            sems = (0, 0) if phase == 0 else (k, 4 - k)
+            remote(ref, ref, wm_s.at[part, sems[0]], wm_r.at[part, sems[1]], peer({(d1, d2)[phase]: k}))
+        for g in range(1, 4) if phase else (0,):
+            expect(
+                (wm_s, part, g), blocks(wm, WTAILS[part], 4 if phase else 3), wm_s.at[part, g], wm_r.at[part, g]
+            )
+
+    def walk_last(part, g):
+        _, d2, d3 = ORDERS[part]
+        if g:
+            got((wm_s, part, g))
+        ref = wm.at[region(part, {d2: (at[d2] + g) % 4, d3: at[d3]}) + WTAILS[part]]
+        for k in (2, 1, 3):
+            remote(ref, ref, wm_s.at[part, 4], wm_r.at[part, 4], peer({d3: k}))
+        if g == 2:
+            expect((wm_s, part, 4), blocks(wm, WTAILS[part], 48), wm_s.at[part, 4], wm_r.at[part, 4])
 
     for part in range(3):
         plane_send(tb, part, tk_s, tk_r)
@@ -159,13 +172,18 @@
     big = ((dg_h, dg), (du_h, du), (dd_h, dd), (eg_h, eg), (eu_h, eu), (ed_h, ed))
     for i, (a, b) in enumerate(big):
         c_w.append(local(a, b.at[core], loc.at[15 + i]))
-    for g in (0, 1, 3, 2):
+    for part in range(3):
+        line_send(tb, part, 0, tk_s, tk_r)
+    c_wm.wait()
+    got(wmx_s)
+    for part in range(3):
+        walk_send(part, 0)
+    for g in (1, 3, 2):
         for part in range(3):
             line_send(tb, part, g, tk_s, tk_r)
-    c_wm.wait()
-    got(wmx_s)
-    for part in range(3):
-        walk_send(wm, part, 0, wm_s, wm_r)
+    for part in range(3):
+        walk_send(part, 1)
+        walk_last(part, 0)
     for i, (a, b) in enumerate(big):
         remote(a, b.at[core], pw_s.at[4 + i], pw_r.at[4 + i], partner)
         expect((pw_s, 4 + i), b.at[0], pw_s.at[4 + i], pw_r.at[4 + i])
@@ -215,8 +233,6 @@
     w64 = wp.reshape(64, 2048)
     w128 = jnp.concatenate([w64[:, :HALF], w64[:, HALF:]], axis=0)
     for part in range(3):
-        walk_send(wm, part, 1, wm_s, wm_r)
-    for part in range(3):
         got((tk_s, part, 4))
     proj = dot_nt(tb.reshape(512, HALF)[...], w128)
     proj = proj + pltpu.roll(pltpu.roll(proj, 508, 0), 64, 1)
@@ -229,8 +245,9 @@
 
     expect(a2_s, rcv.at[0:63], a2_s, a2_r)
     rcv[chip] = msg[chip]
-    for part in range(3):
-        walk_send(wm, part, 2, wm_s, wm_r)
+    for g in (1, 3, 2):
+        for part in range(3):
+            walk_last(part, g)
 
     wd[...] = jnp.zeros_like(wd)
     wdd[...] = jnp.zeros_like(wdd)
@@ -273,7 +290,7 @@
     remote(mx.at[core], mx.at[core], mx_s.at[0], mx_r.at[0], partner)
     expect((mx_s, 0), mx.at[0], mx_s.at[0], mx_r.at[0])
     for part in range(3):
-        got((wm_s, part, 2))
+        got((wm_s, part, 4))
     got((mx_s, 0))
     mxv = mx.reshape(64, 128)
     lhs = jnp.concatenate([mxv[pl.ds(4 * core + i, 8, stride=8), :] for i in range(4)], axis=1).astype(BF16)
@@ -388,6 +405,20 @@
         wait()
 
 
+def closing(a_h, s_h, out_h, nst_h, av, sv, into, out):
+    ins = [pltpu.make_async_copy(s_h.at[t], sv.at[t], into.at[t]) for t in range(4)]
+    ins.append(pltpu.make_async_copy(a_h, av, into.at[4]))
+    outs = [pltpu.make_async_copy(sv.at[t], nst_h.at[t], out.at[t]) for t in range(4)]
+    outs.append(pltpu.make_async_copy(av, out_h, out.at[4]))
+    for cp in ins:
+        cp.start()
+    for cp, back in zip(ins, outs):
+        cp.wait()
+        back.start()
+    for back in outs:
+        back.wait()
+
+
 def per_device(
     tokens, recurrent_state, query_weight, forget_weight, input_weight, outgate_weight, lower_bound, head_gain,
     mixout_weight, first_gain, first_bias, router_weight, branch_vector, dense_gate_weight, dense_up_weight,
@@ -415,14 +446,15 @@
         *[V((4, 3, 4, 8, n), BF16) for n in lanes], *[V((15, 8, n), BF16) for n in lanes],
         *[V((4, 4, 8, n), BF16) for n in lanes],
         V((2, 32, 128), F32), V((2, 4, 2048), F32), V((4, 2048), F32),
-        sem((21,)), sem((4,)), sem((4,)), sem((10,)), sem((10,)), sem((3, 3)), sem((3, 3)), sem(()), sem(()),
+        sem((21,)), sem((4,)), sem((4,)), sem((10,)), sem((10,)), sem((3, 5)), sem((3, 5)), sem(()), sem(()),
         sem((2,)), sem((2,)), sem((3, 5)), sem((3, 5)), sem((3, 5)), sem((3, 5)), sem(()), sem(()), sem((3, 5)), sem((3, 5)),
     ]
     hbm = pl.BlockSpec(memory_space=pltpu.HBM)
     free = pl.BlockSpec(memory_space=pl.ANY)
-    return pl.pallas_call(
+    shapes = (jax.ShapeDtypeStruct((4, 2048), BF16), jax.ShapeDtypeStruct((4, 8, 128, 128), F32))
+    res = pl.pallas_call(
         kernel,
-        out_shape=(jax.ShapeDtypeStruct((4, 2048), BF16), jax.ShapeDtypeStruct((4, 8, 128, 128), F32)),
+        out_shape=shapes,
         in_specs=[hbm] * 22,
         out_specs=(free, free),
         scratch_shapes=scratch,
@@ -431,6 +463,15 @@
         ),
         name="layer",
     )(*args)
+    return pl.pallas_call(
+        closing,
+        out_shape=shapes,
+        in_specs=[free] * 2,
+        out_specs=(free, free),
+        scratch_shapes=[V((4, 2048), BF16), V((4, 8, 128, 128), F32), sem((5,)), sem((5,))],
+        compiler_params=pltpu.CompilerParams(vmem_limit_bytes=60 * 1024 * 1024),
+        name="closing",
+    )(*res)
 
 
 def solution(mesh):

time: 68.7 us -> 64.2 us (0.934)
  local copies, waits for them, and re-layouts: 4.46 us -> 0 us
    unnamed x2 -> x0, local copies, waits for them, and re-layouts: 4.46 us -> none
    pallas_call x1 -> x2, Pallas kernels: 63.3 us -> 63.4 us  [the longest x1 61 us: per_device(): pl.pallas_call(kernel, out_shape=shapes, in_specs=[hbm] * 22, out_specs=(...]
where the time goes in v3:
time: 64.2 us; the launch traced here: 64 us
  Pallas kernels  63.4 us (99%)
  between operations  0.65 us (1%)
    pallas_call x1, Pallas kernels, per_device(): pl.pallas_call(kernel, out_shape=shapes, in_specs=[hbm] * 22, out_specs=(...  61 us
    pallas_call x1, Pallas kernels, per_device(): pl.pallas_call(closing, out_shape=shapes, in_specs=[free] * 2, out_specs=...  2.44 us

profile of v3, /device:TPU:0, one launch (start us, length us, event | category | flops | bytes accessed | tf_op | source)
XLA Modules:
  0.0 64.0 jit_solution(14901487582695877619)
XLA Ops:
  0.6 61.0 %layer.1 = (bf16[4,2048]{1,0:T(4,128)(2,1)}, f32[4,8,128,128]{3,2,1,0:T(8,128)}) custom-call(bf16[4,2048]{1,0:T(4,128)(2,1)} %tok_h.1, f32[4,8,128,128]{3,2,1,0:T(8,128)} %state_h.1, bf16[8,2048]{1,0:T(8,128)(2,1)} %bitcast.22, bf16[8,2048]{1,0:T(8,128)(2,1)} %bitcast.23, bf16[8,2048]{1,0:T(8,128)(2,1)} %bitcast.24, bf16[8,2048]{1,0:T(8,128)(2,1)} %bitcast.25, ...), custom_call_target="tpu_custom_call" | custom-call | tf_op jit(solution)/shard_map/layer/pallas_call | solution.py:455
  61.6 2.4 %closing.1 = (bf16[4,2048]{1,0:T(4,128)(2,1)}, f32[4,8,128,128]{3,2,1,0:T(8,128)}) custom-call(bf16[4,2048]{1,0:T(4,128)(2,1)} %get-tuple-element.4.a_h, f32[4,8,128,128]{3,2,1,0:T(8,128)} %get-tuple-element.5.s_h), custom_call_target="tpu_custom_call" | custom-call | tf_op jit(solution)/shard_map/closing/pallas_call | solution.py:466

commit v4 on v3

--- a/solution.py
+++ b/solution.py
@@ -86,28 +86,19 @@
         pltpu.make_async_copy(ref, ref, sem).wait()
 
     own = (at[0], at[1], at[2])
+    barrier = pltpu.get_barrier_semaphore()
+    for step in [{d: k} for d in range(3) for k in (2, 1, 3)]:
+        pl.semaphore_signal(barrier, inc=1, device_id=(peer(step),), device_id_type=pl.DeviceIdType.MESH)
+    pl.semaphore_signal(barrier, inc=1, device_id=(partner,), device_id_type=pl.DeviceIdType.MESH)
     c_tok = local(tok_h, tokv, loc.at[0])
-    c_wp = [local(w, wp.at[i, core], loc.at[1 + i]) for i, w in enumerate((wq_h, wf_h, wi_h, wo_h))]
     half_own = pl.ds(pl.multiple_of(core * 512, 512), 512)
     c_wm = local(wm_h.at[:, half_own], wm.at[own + (core,)], loc.at[5])
-    c_small = [
-        local(a, b, loc.at[6 + i])
-        for i, (a, b) in enumerate(
-            ((lb_h, lb), (hg_h, hg), (g1_h, g1), (b1_h, b1), (router_h, rt), (branch_h, br),
-             (g2_h, g2), (b2_h, b2), (routes_h, rts))
-        )
-    ]
-    barrier = pltpu.get_barrier_semaphore()
-    steps = [{d1: k1, d2: k2} for d1, d2 in ((0, 1), (0, 2), (1, 2)) for k1 in (2, 1, 3) for k2 in (2, 1, 3)]
-    steps += [{d: k} for d in range(3) for k in (2, 1, 3)]
-    for step in steps:
-        pl.semaphore_signal(barrier, inc=1, device_id=(peer(step),), device_id_type=pl.DeviceIdType.MESH)
-    pl.semaphore_signal(barrier, inc=1, device_id=(partner,), device_id_type=pl.DeviceIdType.MESH)
+    c_wp = [local(w, wp.at[i, core], loc.at[1 + i]) for i, w in enumerate((wq_h, wf_h, wi_h, wo_h))]
     c_tok.wait()
     toks = tokv[...].astype(F32)
     tblk = jnp.concatenate([toks[:, :HALF], toks[:, HALF:]], axis=0).astype(BF16)
     tb[own] = tblk
-    pl.semaphore_wait(barrier, 37)
+    pl.semaphore_wait(barrier, 10)
 
     def region(part, fixed):
         return tuple(fixed.get(d, ALL) for d in range(3))
@@ -119,8 +110,8 @@
     def plane_send(buf, part, ss, rs):
         d1, d2, _ = ORDERS[part]
         ref = buf.at[own + TAILS[part]]
-        for k2 in (2, 1, 3, 0):
-            for k1 in (2, 1, 3, 0):
+        for k2 in (0, 1, 3, 2):
+            for k1 in (1, 3, 2, 0):
                 if k1 or k2:
                     remote(ref, ref, ss.at[part, k2], rs.at[part, (4 - k2) % 4], peer({d1: k1, d2: k2}))
         for g in range(4):
@@ -136,54 +127,61 @@
         if g == 2:
             expect((ss, part, 4), blocks(buf, TAILS[part], 48), ss.at[part, 4], rs.at[part, 4])
 
-    def walk_send(part, phase):
+    def walk_send(buf, tails, part, phase, ss, rs):
         d1, d2, d3 = ORDERS[part]
         if phase:
-            got((wm_s, part, 0))
-        ref = wm.at[region(part, {d: at[d] for d in (d1, d2, d3)[phase:]}) + WTAILS[part]]
+            got((ss, part, 0))
+        ref = buf.at[region(part, {d: at[d] for d in (d1, d2, d3)[phase:]}) + tails[part]]
         for k in (2, 1, 3):
             sems = (0, 0) if phase == 0 else (k, 4 - k)
-            remote(ref, ref, wm_s.at[part, sems[0]], wm_r.at[part, sems[1]], peer({(d1, d2)[phase]: k}))
+            remote(ref, ref, ss.at[part, sems[0]], rs.at[part, sems[1]], peer({(d1, d2)[phase]: k}))
         for g in range(1, 4) if phase else (0,):
-            expect(
-                (wm_s, part, g), blocks(wm, WTAILS[part], 4 if phase else 3), wm_s.at[part, g], wm_r.at[part, g]
-            )
-
-    def walk_last(part, g):
+            expect((ss, part, g), blocks(buf, tails[part], 4 if phase else 3), ss.at[part, g], rs.at[part, g])
+
+    def walk_last(buf, tails, part, g, ss, rs):
         _, d2, d3 = ORDERS[part]
         if g:
-            got((wm_s, part, g))
-        ref = wm.at[region(part, {d2: (at[d2] + g) % 4, d3: at[d3]}) + WTAILS[part]]
+            got((ss, part, g))
+        ref = buf.at[region(part, {d2: (at[d2] + g) % 4, d3: at[d3]}) + tails[part]]
         for k in (2, 1, 3):
-            remote(ref, ref, wm_s.at[part, 4], wm_r.at[part, 4], peer({d3: k}))
+            remote(ref, ref, ss.at[part, 4], rs.at[part, 4], peer({d3: k}))
         if g == 2:
-            expect((wm_s, part, 4), blocks(wm, WTAILS[part], 48), wm_s.at[part, 4], wm_r.at[part, 4])
-
-    for part in range(3):
-        plane_send(tb, part, tk_s, tk_r)
+            expect((ss, part, 4), blocks(buf, tails[part], 48), ss.at[part, 4], rs.at[part, 4])
+
+    of_wm, of_tb = (wm, WTAILS), (tb, TAILS)
+    for part in range(3):
+        walk_send(*of_tb, part, 0, tk_s, tk_r)
     half_in = pl.ds(pl.multiple_of((1 - core) * 512, 512), 512)
     remote(wm_h.at[:, half_in], wm.at[own + (core,)], wmx_s, wmx_r, partner)
     expect(wmx_s, wm.at[own + (0,)], wmx_s, wmx_r)
     for i, w in enumerate((wq_h, wf_h, wi_h, wo_h)):
         remote(w, wp.at[i, core], pw_s.at[i], pw_r.at[i], partner)
         expect((pw_s, i), wp.at[i, 0], pw_s.at[i], pw_r.at[i])
+    c_small = [
+        local(a, b, loc.at[6 + i])
+        for i, (a, b) in enumerate(
+            ((lb_h, lb), (hg_h, hg), (g1_h, g1), (b1_h, b1), (router_h, rt), (branch_h, br),
+             (g2_h, g2), (b2_h, b2), (routes_h, rts))
+        )
+    ]
     c_st = [local(state_h.at[t], st.at[t], stsem.at[t]) for t in range(4)]
     c_w = []
     big = ((dg_h, dg), (du_h, du), (dd_h, dd), (eg_h, eg), (eu_h, eu), (ed_h, ed))
     for i, (a, b) in enumerate(big):
         c_w.append(local(a, b.at[core], loc.at[15 + i]))
     for part in range(3):
-        line_send(tb, part, 0, tk_s, tk_r)
+        walk_send(*of_tb, part, 1, tk_s, tk_r)
+        walk_last(*of_tb, part, 0, tk_s, tk_r)
     c_wm.wait()
     got(wmx_s)
     for part in range(3):
-        walk_send(part, 0)
+        walk_send(*of_wm, part, 0, wm_s, wm_r)
     for g in (1, 3, 2):
         for part in range(3):
-            line_send(tb, part, g, tk_s, tk_r)
-    for part in range(3):
-        walk_send(part, 1)
-        walk_last(part, 0)
+            walk_last(*of_tb, part, g, tk_s, tk_r)
+    for part in range(3):
+        walk_send(*of_wm, part, 1, wm_s, wm_r)
+        walk_last(*of_wm, part, 0, wm_s, wm_r)
     for i, (a, b) in enumerate(big):
         remote(a, b.at[core], pw_s.at[4 + i], pw_r.at[4 + i], partner)
         expect((pw_s, 4 + i), b.at[0], pw_s.at[4 + i], pw_r.at[4 + i])
@@ -247,7 +245,7 @@
     rcv[chip] = msg[chip]
     for g in (1, 3, 2):
         for part in range(3):
-            walk_last(part, g)
+            walk_last(*of_wm, part, g, wm_s, wm_r)
 
     wd[...] = jnp.zeros_like(wd)
     wdd[...] = jnp.zeros_like(wdd)

time: 64.2 us -> 62.9 us (0.980)
  Pallas kernels: 63.4 us -> 62 us
    pallas_call x1, Pallas kernels: 61 us -> 59.6 us  [per_device(): pl.pallas_call(kernel, out_shape=shapes, in_specs=[hbm] * 22, out_specs=(...]
where the time goes in v4:
time: 62.9 us; the launch traced here: 62.7 us
  Pallas kernels  62 us (99%)
  between operations  0.65 us (1%)
    pallas_call x1, Pallas kernels, per_device(): pl.pallas_call(kernel, out_shape=shapes, in_specs=[hbm] * 22, out_specs=(...  59.6 us
    pallas_call x1, Pallas kernels, per_device(): pl.pallas_call(closing, out_shape=shapes, in_specs=[free] * 2, out_specs=...  2.44 us

profile of v4, /device:TPU:0, one launch (start us, length us, event | category | flops | bytes accessed | tf_op | source)
XLA Modules:
  0.0 62.7 jit_solution(9972849604431409328)
XLA Ops:
  0.6 59.6 %layer.1 = (bf16[4,2048]{1,0:T(4,128)(2,1)}, f32[4,8,128,128]{3,2,1,0:T(8,128)}) custom-call(bf16[4,2048]{1,0:T(4,128)(2,1)} %tok_h.1, f32[4,8,128,128]{3,2,1,0:T(8,128)} %state_h.1, bf16[8,2048]{1,0:T(8,128)(2,1)} %bitcast.22, bf16[8,2048]{1,0:T(8,128)(2,1)} %bitcast.23, bf16[8,2048]{1,0:T(8,128)(2,1)} %bitcast.24, bf16[8,2048]{1,0:T(8,128)(2,1)} %bitcast.25, ...), custom_call_target="tpu_custom_call" | custom-call | tf_op jit(solution)/shard_map/layer/pallas_call | solution.py:453
  60.2 2.4 %closing.1 = (bf16[4,2048]{1,0:T(4,128)(2,1)}, f32[4,8,128,128]{3,2,1,0:T(8,128)}) custom-call(bf16[4,2048]{1,0:T(4,128)(2,1)} %get-tuple-element.4.a_h, f32[4,8,128,128]{3,2,1,0:T(8,128)} %get-tuple-element.5.s_h), custom_call_target="tpu_custom_call" | custom-call | tf_op jit(solution)/shard_map/closing/pallas_call | solution.py:464

commit v5 on v4

--- a/solution.py
+++ b/solution.py
@@ -47,7 +47,7 @@
     out_h, nst_h,
     tokv, outv, st, nst, wp, lb, hg, wm, g1, b1, rt, br, dg, du, dd, eg, eu, ed, g2, b2, rts,
     tb, nb, msg, rcv, ob, xe, wd, wdd, rd,
-    r1a, r1b, r1c, r2a, r2b, r2c, t1a, t1b, t1c, mx, mos, mor,
+    r1a, r1b, r1c, r2a, r2b, r2c, t1a, t1b, t1c, mx, mos, mor, egt, eut,
     loc, stsem, nsem, pw_s, pw_r, wm_s, wm_r, wmx_s, wmx_r, mx_s, mx_r, tk_s, tk_r, nb_s, nb_r, a2_s, a2_r, rs_s, rs_r,
 ):
     me = lax.axis_index("ep")
@@ -86,6 +86,8 @@
         pltpu.make_async_copy(ref, ref, sem).wait()
 
     own = (at[0], at[1], at[2])
+    four = pl.ds(0, 4)
+    rcv[...] = jnp.zeros_like(rcv)
     barrier = pltpu.get_barrier_semaphore()
     for step in [{d: k} for d in range(3) for k in (2, 1, 3)]:
         pl.semaphore_signal(barrier, inc=1, device_id=(peer(step),), device_id_type=pl.DeviceIdType.MESH)
@@ -169,13 +171,13 @@
     big = ((dg_h, dg), (du_h, du), (dd_h, dd), (eg_h, eg), (eu_h, eu), (ed_h, ed))
     for i, (a, b) in enumerate(big):
         c_w.append(local(a, b.at[core], loc.at[15 + i]))
+    c_wm.wait()
+    got(wmx_s)
+    for part in range(3):
+        walk_send(*of_wm, part, 0, wm_s, wm_r)
     for part in range(3):
         walk_send(*of_tb, part, 1, tk_s, tk_r)
         walk_last(*of_tb, part, 0, tk_s, tk_r)
-    c_wm.wait()
-    got(wmx_s)
-    for part in range(3):
-        walk_send(*of_wm, part, 0, wm_s, wm_r)
     for g in (1, 3, 2):
         for part in range(3):
             walk_last(*of_tb, part, g, tk_s, tk_r)
@@ -225,6 +227,13 @@
     s_row, s_col = iota((32, 512), 0), iota((32, 512), 1)
     fold = jnp.where((s_col // 64 == s_row % 8) & (s_col % 8 == s_row // 8), 1.0, 0.0).astype(BF16)
 
+    def turn(c):
+        egt[c] = jnp.transpose(eg[c])
+        eut[c] = jnp.transpose(eu[c])
+
+    for i in range(6):
+        c_w[i].wait()
+    turn(core)
     for i in range(4):
         c_wp[i].wait()
         got((pw_s, i))
@@ -239,10 +248,10 @@
     @pl.loop(1, 64)
     def _(j):
         to = (chip + j) % 64
-        remote(msg.at[to], rcv.at[chip], a2_s, a2_r, 2 * to + core)
-
-    expect(a2_s, rcv.at[0:63], a2_s, a2_r)
-    rcv[chip] = msg[chip]
+        remote(msg.at[to, four], rcv.at[chip, four], a2_s, a2_r, 2 * to + core)
+
+    expect(a2_s, rcv.at[0:63, four], a2_s, a2_r)
+    rcv[chip, four] = msg[chip, four]
     for g in (1, 3, 2):
         for part in range(3):
             walk_last(*of_wm, part, g, wm_s, wm_r)
@@ -250,7 +259,6 @@
     wd[...] = jnp.zeros_like(wd)
     wdd[...] = jnp.zeros_like(wdd)
     for i in range(6):
-        c_w[i].wait()
         got((pw_s, 4 + i))
     for c in range(2):
         for h in range(2):
@@ -309,6 +317,7 @@
 
     for part in range(3):
         plane_send(nb, part, nb_s, nb_r)
+    turn(1 - core)
     for g in (0, 1, 3, 2):
         for part in range(3):
             line_send(nb, part, g, nb_s, nb_r)
@@ -320,9 +329,12 @@
         sel = dot(sels[u], nbv[256 * u : 256 * (u + 1), :]).astype(BF16)
         xe[64 * u : 64 * (u + 1), :HALF] = sel[:64]
         xe[64 * u : 64 * (u + 1), HALF:] = sel[64:]
-    gate = dot_nt(xe[...], eg.reshape(896, 2048)[...])
-    up = dot_nt(xe[...], eu.reshape(896, 2048)[...])
-    hidden = (gate * sigmoid(gate) * up).astype(BF16)
+    xes = xe[...]
+    hiddens = []
+    for c in range(2):
+        gate = dot(xes, egt[c])
+        up = dot(xes, eut[c])
+        hiddens.append((gate * sigmoid(gate) * up).astype(BF16))
     y2 = dot_nt(nbv[...], wd[...])
     first_half = (iota((512, 256), 0) // 4) % 2 == 0
     y = jnp.where(first_half, y2[:, :256], y2[:, 256:]).reshape(64, 8, 256)
@@ -333,7 +345,7 @@
     hd = yg * sigmoid(yg) * y[:, 128:] * branch
     top = (iota((512, 128), 0) // 4) % 2 == 0
     hdd = jnp.concatenate([jnp.where(top, hd, 0.0), jnp.where(top, 0.0, hd)], axis=1).astype(BF16)
-    slots = dot(hidden, ed.reshape(896, 2048)[...]).astype(BF16)
+    slots = (dot(hiddens[0], ed[0]) + dot(hiddens[1], ed[1])).astype(BF16)
     obv = ob.reshape(512, HALF)
     for u in range(2):
         ru = slice(256 * u, 256 * (u + 1))
@@ -443,7 +455,7 @@
         V((32, 128), F32),
         *[V((4, 3, 4, 8, n), BF16) for n in lanes], *[V((15, 8, n), BF16) for n in lanes],
         *[V((4, 4, 8, n), BF16) for n in lanes],
-        V((2, 32, 128), F32), V((2, 4, 2048), F32), V((4, 2048), F32),
+        V((2, 32, 128), F32), V((2, 4, 2048), F32), V((4, 2048), F32), V((2, 2048, 448), BF16), V((2, 2048, 448), BF16),
         sem((21,)), sem((4,)), sem((4,)), sem((10,)), sem((10,)), sem((3, 5)), sem((3, 5)), sem(()), sem(()),
         sem((2,)), sem((2,)), sem((3, 5)), sem((3, 5)), sem((3, 5)), sem((3, 5)), sem(()), sem(()), sem((3, 5)), sem((3, 5)),
     ]

time: 62.9 us -> 61.6 us (0.979)
  Pallas kernels: 62 us -> 60.8 us
    pallas_call x1, Pallas kernels: 59.6 us -> 58.3 us  [per_device(): pl.pallas_call(kernel, out_shape=shapes, in_specs=[hbm] * 22, out_specs=(...]
where the time goes in v5:
time: 61.6 us; the launch traced here: 61.4 us
  Pallas kernels  60.8 us (99%)
  between operations  0.65 us (1%)
    pallas_call x1, Pallas kernels, per_device(): pl.pallas_call(kernel, out_shape=shapes, in_specs=[hbm] * 22, out_specs=(...  58.3 us
    pallas_call x1, Pallas kernels, per_device(): pl.pallas_call(closing, out_shape=shapes, in_specs=[free] * 2, out_specs=...  2.44 us

profile of v5, /device:TPU:0, one launch (start us, length us, event | category | flops | bytes accessed | tf_op | source)
XLA Modules:
  0.0 61.4 jit_solution(7649770417469486084)
XLA Ops:
  0.6 58.3 %layer.1 = (bf16[4,2048]{1,0:T(4,128)(2,1)}, f32[4,8,128,128]{3,2,1,0:T(8,128)}) custom-call(bf16[4,2048]{1,0:T(4,128)(2,1)} %tok_h.1, f32[4,8,128,128]{3,2,1,0:T(8,128)} %state_h.1, bf16[8,2048]{1,0:T(8,128)(2,1)} %bitcast.22, bf16[8,2048]{1,0:T(8,128)(2,1)} %bitcast.23, bf16[8,2048]{1,0:T(8,128)(2,1)} %bitcast.24, bf16[8,2048]{1,0:T(8,128)(2,1)} %bitcast.25, ...), custom_call_target="tpu_custom_call" | custom-call | tf_op jit(solution)/shard_map/layer/pallas_call | solution.py:465
  59.0 2.4 %closing.1 = (bf16[4,2048]{1,0:T(4,128)(2,1)}, f32[4,8,128,128]{3,2,1,0:T(8,128)}) custom-call(bf16[4,2048]{1,0:T(4,128)(2,1)} %get-tuple-element.4.a_h, f32[4,8,128,128]{3,2,1,0:T(8,128)} %get-tuple-element.5.s_h), custom_call_target="tpu_custom_call" | custom-call | tf_op jit(solution)/shard_map/closing/pallas_call | solution.py:476

commit v6 on v5

--- a/solution.py
+++ b/solution.py
@@ -151,11 +151,11 @@
             expect((ss, part, 4), blocks(buf, tails[part], 48), ss.at[part, 4], rs.at[part, 4])
 
     of_wm, of_tb = (wm, WTAILS), (tb, TAILS)
-    for part in range(3):
-        walk_send(*of_tb, part, 0, tk_s, tk_r)
     half_in = pl.ds(pl.multiple_of((1 - core) * 512, 512), 512)
     remote(wm_h.at[:, half_in], wm.at[own + (core,)], wmx_s, wmx_r, partner)
     expect(wmx_s, wm.at[own + (0,)], wmx_s, wmx_r)
+    for part in range(3):
+        walk_send(*of_tb, part, 0, tk_s, tk_r)
     for i, w in enumerate((wq_h, wf_h, wi_h, wo_h)):
         remote(w, wp.at[i, core], pw_s.at[i], pw_r.at[i], partner)
         expect((pw_s, i), wp.at[i, 0], pw_s.at[i], pw_r.at[i])
@@ -258,7 +258,7 @@
 
     wd[...] = jnp.zeros_like(wd)
     wdd[...] = jnp.zeros_like(wdd)
-    for i in range(6):
+    for i in range(3):
         got((pw_s, 4 + i))
     for c in range(2):
         for h in range(2):
@@ -317,6 +317,8 @@
 
     for part in range(3):
         plane_send(nb, part, nb_s, nb_r)
+    for i in range(3, 6):
+        got((pw_s, 4 + i))
     turn(1 - core)
     for g in (0, 1, 3, 2):
         for part in range(3):

time: 61.6 us -> 61.6 us (level)
  no operation moved by 1% of the time
where the time goes in v6:
time: 61.6 us; the launch traced here: 61.4 us
  Pallas kernels  60.7 us (99%)
  between operations  0.65 us (1%)
    pallas_call x1, Pallas kernels, per_device(): pl.pallas_call(kernel, out_shape=shapes, in_specs=[hbm] * 22, out_specs=(...  58.3 us
    pallas_call x1, Pallas kernels, per_device(): pl.pallas_call(closing, out_shape=shapes, in_specs=[free] * 2, out_specs=...  2.44 us

profile of v6, /device:TPU:0, one launch (start us, length us, event | category | flops | bytes accessed | tf_op | source)
XLA Modules:
  0.0 61.4 jit_solution(11055467725140240722)
XLA Ops:
  0.6 58.3 %layer.1 = (bf16[4,2048]{1,0:T(4,128)(2,1)}, f32[4,8,128,128]{3,2,1,0:T(8,128)}) custom-call(bf16[4,2048]{1,0:T(4,128)(2,1)} %tok_h.1, f32[4,8,128,128]{3,2,1,0:T(8,128)} %state_h.1, bf16[8,2048]{1,0:T(8,128)(2,1)} %bitcast.22, bf16[8,2048]{1,0:T(8,128)(2,1)} %bitcast.23, bf16[8,2048]{1,0:T(8,128)(2,1)} %bitcast.24, bf16[8,2048]{1,0:T(8,128)(2,1)} %bitcast.25, ...), custom_call_target="tpu_custom_call" | custom-call | tf_op jit(solution)/shard_map/layer/pallas_call | solution.py:467
  58.9 2.4 %closing.1 = (bf16[4,2048]{1,0:T(4,128)(2,1)}, f32[4,8,128,128]{3,2,1,0:T(8,128)}) custom-call(bf16[4,2048]{1,0:T(4,128)(2,1)} %get-tuple-element.4.a_h, f32[4,8,128,128]{3,2,1,0:T(8,128)} %get-tuple-element.5.s_h), custom_call_target="tpu_custom_call" | custom-call | tf_op jit(solution)/shard_map/closing/pallas_call | solution.py:478
